TPU v7x, 256 devices: a whole 4x4x8 slice. The times are simulated.
256 devices in a mesh: kv: 64 (over z, y, core), tp: 4 (over x).
Axes of the slice: x: 4, y: 4, z: 8, core: 2. Of those that a mesh axis runs over, the one named last changes fastest.
Arguments:
- queries: bfloat16 [24576, 2048], P('kv', 'tp'), may hold values from -3 to 3
- key_heads: bfloat16 [24576, 512], P('kv', 'tp'), may hold values from -3 to 3
- values: bfloat16 [24576, 512], P('kv', 'tp'), may hold values from -6 to 6
- log_sums: float32 [32, 24576], P('tp', 'kv'), may hold values from 4 to 6
- out_grad: bfloat16 [24576, 2048], P('kv', 'tp'), may hold values from -12 to 12
- inputs: bfloat16 [24576, 4096], P('kv', 'tp'), may hold values from -0.059814453 to 0.059814453
- chosen: int32 [8, 384, 16], P('tp'), may hold values from -1 to 383, as said below
Outputs:
- query_grad: float32 [24576, 2048], P('kv', 'tp')
- key_grad: float32 [24576, 512], P('kv', 'tp')
- value_grad: float32 [24576, 512], P('kv', 'tp')
- weight_grad: float32 [4096, 512], P('kv', 'tp')
Inputs may be any that keep to these rules, and one draw needn't show every extreme that they name: `chosen`: for each key-value head and query block the used entries come first, are distinct, and none is above the query block's own number; -1 fills the rest. Up to 16 entries are used, all of them in some query blocks. For one key-value head, the query blocks held by one index of kv list at most one block of each other index of kv, and every index of kv but the first lists a block of the first.
All inputs are finite; a program needn't handle non-finite values.
Results may differ from a plain program's by a relative error of at most 0.014.
Values may be sent and summed in bfloat16 or wider, within the bound.
No kernel may reach another device: no remote copies, remote signals or barrier semaphores. Data moves between devices by JAX's collectives and lax.ppermute only.
A program may use at most 128 MiB of HBM per device.

v0:
```python
import jax
import jax.numpy as jnp
from jax import lax
from jax.sharding import PartitionSpec as P

HD = 64
BLOCK = 64


def split_up(array, dim, count):
    lengths = array.shape
    pieces = array.reshape(*lengths[:dim], count, lengths[dim] // count, *lengths[dim + 1 :])
    return jnp.moveaxis(pieces, dim, 0)


def sum_at_owner(array, axis, dim):
    pieces = split_up(array, dim, lax.axis_size(axis))
    arrived = lax.all_to_all(pieces, axis, split_axis=0, concat_axis=0, tiled=True)
    return arrived.astype(jnp.float32).sum(axis=0)


def local(queries, key_heads, values, log_sums, out_grad, inputs, chosen):
    device_count = lax.axis_size("kv")
    my_index = lax.axis_index("kv")
    local_rows = queries.shape[0]
    blocks_here = local_rows // BLOCK
    groups_here = key_heads.shape[1] // HD
    heads_here = log_sums.shape[0]
    per_group = heads_here // groups_here
    list_size = chosen.shape[2]
    scaling = HD ** (-0.5)
    kv_pairs = jnp.concatenate(
        [
            key_heads.reshape(local_rows, groups_here, HD),
            values.reshape(local_rows, groups_here, HD),
        ],
        axis=2,
    )
    own_blocks = kv_pairs.reshape(blocks_here, BLOCK, groups_here, 2 * HD)
    my_lists = lax.dynamic_slice_in_dim(chosen, my_index * blocks_here, blocks_here, 1)
    offsets = jnp.arange(blocks_here, dtype=jnp.int32)
    other_devs = (jnp.arange(device_count) != my_index)[None, :, None]
    asked_for = chosen.reshape(groups_here, device_count, blocks_here * list_size)[..., None]
    asked_for = jnp.any(asked_for == my_index * blocks_here + offsets, axis=2) & other_devs
    outgoing = jnp.einsum(
        "grb,bkgc->rkgc",
        asked_for.astype(jnp.bfloat16),
        own_blocks,
        preferred_element_type=jnp.float32,
    ).astype(jnp.bfloat16)
    remote = lax.all_to_all(outgoing, "kv", split_axis=0, concat_axis=0, tiled=True)
    key_table = jnp.concatenate([remote, own_blocks], axis=0)
    owner_dev = my_lists // blocks_here
    is_valid = my_lists >= 0
    source = jnp.where(
        owner_dev == my_index, device_count + my_lists % blocks_here, jnp.maximum(owner_dev, 0)
    )
    group_col = jnp.arange(groups_here, dtype=jnp.int32)[:, None]
    key_offsets = jnp.arange(BLOCK, dtype=jnp.int32)

    def one_block(totals, position):
        slot_index = lax.dynamic_index_in_dim(source, position, 1, keepdims=False)
        block_list = lax.dynamic_index_in_dim(my_lists, position, 1, keepdims=False)
        list_valid = lax.dynamic_index_in_dim(is_valid, position, 1, keepdims=False)
        fetched = key_table[slot_index, :, group_col, :].reshape(
            groups_here, list_size * BLOCK, 2 * HD
        )
        key_part = fetched[..., :HD]
        value_part = fetched[..., HD:]
        first_row = position * BLOCK
        query_part = lax.dynamic_slice_in_dim(queries, first_row, BLOCK, 0).reshape(
            BLOCK, groups_here, per_group, HD
        )
        grad_part = lax.dynamic_slice_in_dim(out_grad, first_row, BLOCK, 0).reshape(
            BLOCK, groups_here, per_group, HD
        )
        sums_part = lax.dynamic_slice_in_dim(log_sums, first_row, BLOCK, 1).reshape(
            groups_here, per_group, BLOCK
        )
        scores = (
            jnp.einsum("igrd,gkd->grik", query_part, key_part, preferred_element_type=jnp.float32)
            * scaling
        )
        key_pos = (jnp.maximum(block_list, 0)[:, :, None] * BLOCK + key_offsets).reshape(
            groups_here, -1
        )
        key_valid = jnp.repeat(list_valid, BLOCK, axis=1)
        query_pos = (my_index * blocks_here + position) * BLOCK + key_offsets
        visible = key_valid[:, None, None, :] & (
            key_pos[:, None, None, :] <= query_pos[None, None, :, None]
        )
        prob_rows = jnp.where(visible, jnp.exp(scores - sums_part[..., None]), 0.0)
        prob_grad = jnp.einsum(
            "igrd,gkd->grik", grad_part, value_part, preferred_element_type=jnp.float32
        )
        row_delta = jnp.sum(prob_rows * prob_grad, axis=-1, keepdims=True)
        score_grad = prob_rows * (prob_grad - row_delta)
        prob_half = prob_rows.astype(jnp.bfloat16)
        score_half = score_grad.astype(jnp.bfloat16)
        query_part_grad = (
            jnp.einsum("grik,gkd->igrd", score_half, key_part, preferred_element_type=jnp.float32)
            * scaling
        )
        key_contrib = (
            jnp.einsum("grik,igrd->gkd", score_half, query_part, preferred_element_type=jnp.float32)
            * scaling
        )
        value_contrib = jnp.einsum(
            "grik,igrd->gkd", prob_half, grad_part, preferred_element_type=jnp.float32
        )
        contribs = jnp.concatenate([key_contrib, value_contrib], axis=2).reshape(
            groups_here, list_size, BLOCK, 2 * HD
        )
        totals = totals.at[slot_index, :, group_col, :].add(contribs)
        return (totals, query_part_grad.reshape(BLOCK, heads_here * HD))

    start_totals = jnp.zeros((device_count + blocks_here, BLOCK, groups_here, 2 * HD), jnp.float32)
    totals, query_blocks = lax.scan(
        one_block, start_totals, jnp.arange(blocks_here, dtype=jnp.int32)
    )
    query_grad = query_blocks.reshape(local_rows, heads_here * HD)
    returned = lax.all_to_all(
        totals[:device_count].astype(jnp.bfloat16), "kv", split_axis=0, concat_axis=0, tiled=True
    ).astype(jnp.float32)
    summed = totals[device_count:] + jnp.einsum(
        "grb,rkgc->bkgc", asked_for.astype(jnp.float32), returned, precision=lax.Precision.HIGHEST
    )
    summed = summed.reshape(local_rows, groups_here, 2 * HD)
    key_grad = summed[..., :HD].reshape(local_rows, groups_here * HD)
    value_grad = summed[..., HD:].reshape(local_rows, groups_here * HD)
    whole_inputs = lax.all_gather(inputs, "tp", axis=1, tiled=True)
    key_half = key_grad.astype(jnp.bfloat16)
    weight_grad = sum_at_owner(
        lax.dot_general(
            whole_inputs, key_half, (((0,), (0,)), ((), ())), preferred_element_type=jnp.float32
        ).astype(jnp.bfloat16),
        "kv",
        0,
    )
    return (query_grad, key_grad, value_grad, weight_grad)


def solution(mesh):
    placed = (
        P("kv", "tp"),
        P("kv", "tp"),
        P("kv", "tp"),
        P("tp", "kv"),
        P("kv", "tp"),
        P("kv", "tp"),
        P("tp", None, None),
    )
    return jax.shard_map(
        local,
        mesh=mesh,
        in_specs=placed,
        out_specs=(P("kv", "tp"), P("kv", "tp"), P("kv", "tp"), P("kv", "tp")),
        check_vma=False,
    )
```

profile of v0, /device:TPU:1, one launch (start us, length us, event | category | flops | bytes accessed | tf_op | source)
XLA Modules:
  0.0 308.7 jit_solution(11476069297831048445)
XLA Ops:
  7.2 1.0 copy.71
  8.3 1.0 concatenate.22
  9.5 1.0 concatenate.23
  11.9 2.7 copy.72
  14.6 13.2 %all-to-all-start = ((bf16[64,64,2,128]{3,1,2,0:T(8,128)(2,1)}), bf16[64,64,2,128]{3,1,2,0:T(8,128)(2,1)S(1)}, u32[]{:S(2)}, u32[]{:S(2)}) async-start(bf16[64,64,2,128]{3,1,2,0:T(8,128)(2,1)} %copy.72), calls=%async_computation | async-start | bytes 4194304 | tf_op jit(solution)/shard_map/all_to_all | solution.py:51
  29.6 47.9 %all-to-all-done = bf16[64,64,2,128]{3,1,2,0:T(8,128)(2,1)S(1)} async-done(((bf16[64,64,2,128]{3,1,2,0:T(8,128)(2,1)}), bf16[64,64,2,128]{3,1,2,0:T(8,128)(2,1)S(1)}, u32[]{:S(2)}, u32[]{:S(2)}) %all-to-all-start) | async-done | bytes 2097184 | tf_op jit(solution)/shard_map/all_to_all | solution.py:51
  77.5 1.6 pad_maximum_fusion.1
  79.1 2.7 broadcast_in_dim.53
  81.8 117.4 %while.16 = (s32[]{:T(128)}, f32[70,64,2,128]{3,1,2,0:T(8,128)}, f32[6,64,512]{2,1,0:T(8,128)}, s32[6]{0:T(128)S(1)}, s32[2,6,16]{2,0,1:T(2,128)S(1)}, /*index=5...) while((s32[]{:T(128)}, f32[70,64,2,128]{3,1,2,0:T(8,128)}, ...), condition=%wide.region_4.5_spmd.clone.clone, body=%wide.region_1.4_spmd.clone.clone.sunk | while | flops 341215168 | bytes 32724180 | solution.py:118
  83.0 0.9 constant_dynamic-slice_fusion.8
  86.2 2.3 gather_fusion
  93.7 6.5 %scatter_fusion = f32[70,64,2,128]{3,1,2,0:T(8,128)} fusion(f32[70,64,2,128]{3,1,2,0:T(8,128)} %get-tuple-element.400, s32[32]{0:T(128)S(1)} %reshape.219, f32[32,64,128]{2,1,0:T(8,128)S(1)} %bitcast.142), kind=kCustom, calls=%fused_computation.1.clone.clone.1 | custom fusion | flops 262144 | bytes 3145984 | tf_op jit(solution)/shard_map/while/body/eval_jaxpr/scatter-add | solution.py:114
  102.9 0.9 constant_dynamic-slice_fusion.8
  106.0 2.3 gather_fusion
  113.6 6.4 %scatter_fusion = f32[70,64,2,128]{3,1,2,0:T(8,128)} fusion(f32[70,64,2,128]{3,1,2,0:T(8,128)} %get-tuple-element.400, s32[32]{0:T(128)S(1)} %reshape.219, f32[32,64,128]{2,1,0:T(8,128)S(1)} %bitcast.142), kind=kCustom, calls=%fused_computation.1.clone.clone.1 | custom fusion | flops 262144 | bytes 3145984 | tf_op jit(solution)/shard_map/while/body/eval_jaxpr/scatter-add | solution.py:114
  125.8 2.3 gather_fusion
  133.4 6.3 %scatter_fusion = f32[70,64,2,128]{3,1,2,0:T(8,128)} fusion(f32[70,64,2,128]{3,1,2,0:T(8,128)} %get-tuple-element.400, s32[32]{0:T(128)S(1)} %reshape.219, f32[32,64,128]{2,1,0:T(8,128)S(1)} %bitcast.142), kind=kCustom, calls=%fused_computation.1.clone.clone.1 | custom fusion | flops 262144 | bytes 3145984 | tf_op jit(solution)/shard_map/while/body/eval_jaxpr/scatter-add | solution.py:114
  145.5 2.3 gather_fusion
  153.0 6.2 %scatter_fusion = f32[70,64,2,128]{3,1,2,0:T(8,128)} fusion(f32[70,64,2,128]{3,1,2,0:T(8,128)} %get-tuple-element.400, s32[32]{0:T(128)S(1)} %reshape.219, f32[32,64,128]{2,1,0:T(8,128)S(1)} %bitcast.142), kind=kCustom, calls=%fused_computation.1.clone.clone.1 | custom fusion | flops 262144 | bytes 3145984 | tf_op jit(solution)/shard_map/while/body/eval_jaxpr/scatter-add | solution.py:114
  165.0 2.3 gather_fusion
  172.5 6.0 %scatter_fusion = f32[70,64,2,128]{3,1,2,0:T(8,128)} fusion(f32[70,64,2,128]{3,1,2,0:T(8,128)} %get-tuple-element.400, s32[32]{0:T(128)S(1)} %reshape.219, f32[32,64,128]{2,1,0:T(8,128)S(1)} %bitcast.142), kind=kCustom, calls=%fused_computation.1.clone.clone.1 | custom fusion | flops 262144 | bytes 3145984 | tf_op jit(solution)/shard_map/while/body/eval_jaxpr/scatter-add | solution.py:114
  184.4 2.3 gather_fusion
  191.9 5.9 %scatter_fusion = f32[70,64,2,128]{3,1,2,0:T(8,128)} fusion(f32[70,64,2,128]{3,1,2,0:T(8,128)} %get-tuple-element.400, s32[32]{0:T(128)S(1)} %reshape.219, f32[32,64,128]{2,1,0:T(8,128)S(1)} %bitcast.142), kind=kCustom, calls=%fused_computation.1.clone.clone.1 | custom fusion | flops 262144 | bytes 3145984 | tf_op jit(solution)/shard_map/while/body/eval_jaxpr/scatter-add | solution.py:114
  199.2 4.1 %slice.48 = bf16[64,64,2,128]{3,1,2,0:T(8,128)(2,1)} slice(f32[70,64,2,128]{3,1,2,0:T(8,128)} %get-tuple-element.169), slice={[0:64], [0:64], [0:2], [0:128]} | slice | bytes 4194304 | tf_op jit(solution)/shard_map/slice | solution.py:123
  203.3 6.2 %all-to-all-start.1 = ((bf16[64,64,2,128]{3,1,2,0:T(8,128)(2,1)}), bf16[64,64,2,128]{3,1,2,0:T(8,128)(2,1)S(1)}, u32[]{:S(2)}, u32[]{:S(2)}) async-start(bf16[64,64,2,128]{3,1,2,0:T(8,128)(2,1)} %slice.48), calls=%async_computation.1 | async-start | bytes 4194304 | tf_op jit(solution)/shard_map/all_to_all | solution.py:122
  209.5 7.1 %copy.75 = f32[70,64,2,128]{3,0,1,2:T(8,128)} copy(f32[70,64,2,128]{3,1,2,0:T(8,128)} %get-tuple-element.169) | data formatting | bytes 9175040 | tf_op jit(solution)/shard_map/while | solution.py:118
  216.6 42.9 %all-to-all-done.1 = bf16[64,64,2,128]{3,1,2,0:T(8,128)(2,1)S(1)} async-done(((bf16[64,64,2,128]{3,1,2,0:T(8,128)(2,1)}), bf16[64,64,2,128]{3,1,2,0:T(8,128)(2,1)S(1)}, u32[]{:S(2)}, u32[]{:S(2)}) %all-to-all-start.1) | async-done | bytes 2097184 | tf_op jit(solution)/shard_map/all_to_all | solution.py:122
  259.5 2.3 fusion.24
  262.2 2.6 fusion.18
  264.8 1.3 copy.80
  266.2 6.8 %all-to-all-start.2 = ((bf16[64,64,128]{2,1,0:T(8,128)(2,1)}), bf16[64,64,128]{2,1,0:T(8,128)(2,1)S(1)}, u32[]{:S(2)}, u32[]{:S(2)}) async-start(bf16[64,64,128]{2,1,0:T(8,128)(2,1)} %bitcast.10), calls=%async_computation.2 | async-start | bytes 2097152 | tf_op jit(solution)/shard_map/all_to_all | solution.py:18
  274.7 26.4 %all-to-all-done.2 = bf16[64,64,128]{2,1,0:T(8,128)(2,1)S(1)} async-done(((bf16[64,64,128]{2,1,0:T(8,128)(2,1)}), bf16[64,64,128]{2,1,0:T(8,128)(2,1)S(1)}, u32[]{:S(2)}, u32[]{:S(2)}) %all-to-all-start.2) | async-done | bytes 1048608 | tf_op jit(solution)/shard_map/all_to_all | solution.py:18
  (233 shorter events, 50.3 us)
Async XLA Ops:
  14.6 62.9 %all-to-all-start = ((bf16[64,64,2,128]{3,1,2,0:T(8,128)(2,1)}), bf16[64,64,2,128]{3,1,2,0:T(8,128)(2,1)S(1)}, u32[]{:S(2)}, u32[]{:S(2)}) async-start(bf16[64,64,2,128]{3,1,2,0:T(8,128)(2,1)} %copy.72), calls=%async_computation | async-start | bytes 4194304 | tf_op jit(solution)/shard_map/all_to_all | solution.py:51
  27.8 234.4 %all-gather.2.cloned.1.call-start = ((), (), s32[]{:S(2)}) async-start(), calls=%async_computation.3 | async-start | bytes 3932160 | tf_op jit(solution)/shard_map/all_gather | solution.py:131
  88.5 3.6 %copy-start = (bf16[32,64,128]{2,1,0:T(8,128)(2,1)}, bf16[32,64,128]{2,1,0:T(8,128)(2,1)S(1)}, u32[]{:S(2)}) copy-start(bf16[32,64,128]{2,1,0:T(8,128)(2,1)S(1)} %gather_fusion) | copy-start | bytes 1572868 | tf_op jit(solution)/shard_map/while
  93.6 6.6 %copy-start.1 = (bf16[32,64,128]{2,1,0:T(8,128)(2,1)S(1)}, bf16[32,64,128]{2,1,0:T(8,128)(2,1)}, u32[]{:S(2)}) copy-start(bf16[32,64,128]{2,1,0:T(8,128)(2,1)} %copy-done) | copy-start | bytes 1572868 | tf_op jit(solution)/shard_map/while
  108.4 3.6 %copy-start = (bf16[32,64,128]{2,1,0:T(8,128)(2,1)}, bf16[32,64,128]{2,1,0:T(8,128)(2,1)S(1)}, u32[]{:S(2)}) copy-start(bf16[32,64,128]{2,1,0:T(8,128)(2,1)S(1)} %gather_fusion) | copy-start | bytes 1572868 | tf_op jit(solution)/shard_map/while
  113.5 6.5 %copy-start.1 = (bf16[32,64,128]{2,1,0:T(8,128)(2,1)S(1)}, bf16[32,64,128]{2,1,0:T(8,128)(2,1)}, u32[]{:S(2)}) copy-start(bf16[32,64,128]{2,1,0:T(8,128)(2,1)} %copy-done) | copy-start | bytes 1572868 | tf_op jit(solution)/shard_map/while
  128.1 3.6 %copy-start = (bf16[32,64,128]{2,1,0:T(8,128)(2,1)}, bf16[32,64,128]{2,1,0:T(8,128)(2,1)S(1)}, u32[]{:S(2)}) copy-start(bf16[32,64,128]{2,1,0:T(8,128)(2,1)S(1)} %gather_fusion) | copy-start | bytes 1572868 | tf_op jit(solution)/shard_map/while
  133.3 6.4 %copy-start.1 = (bf16[32,64,128]{2,1,0:T(8,128)(2,1)S(1)}, bf16[32,64,128]{2,1,0:T(8,128)(2,1)}, u32[]{:S(2)}) copy-start(bf16[32,64,128]{2,1,0:T(8,128)(2,1)} %copy-done) | copy-start | bytes 1572868 | tf_op jit(solution)/shard_map/while
  147.8 3.6 %copy-start = (bf16[32,64,128]{2,1,0:T(8,128)(2,1)}, bf16[32,64,128]{2,1,0:T(8,128)(2,1)S(1)}, u32[]{:S(2)}) copy-start(bf16[32,64,128]{2,1,0:T(8,128)(2,1)S(1)} %gather_fusion) | copy-start | bytes 1572868 | tf_op jit(solution)/shard_map/while
  152.9 6.3 %copy-start.1 = (bf16[32,64,128]{2,1,0:T(8,128)(2,1)S(1)}, bf16[32,64,128]{2,1,0:T(8,128)(2,1)}, u32[]{:S(2)}) copy-start(bf16[32,64,128]{2,1,0:T(8,128)(2,1)} %copy-done) | copy-start | bytes 1572868 | tf_op jit(solution)/shard_map/while
  167.3 3.6 %copy-start = (bf16[32,64,128]{2,1,0:T(8,128)(2,1)}, bf16[32,64,128]{2,1,0:T(8,128)(2,1)S(1)}, u32[]{:S(2)}) copy-start(bf16[32,64,128]{2,1,0:T(8,128)(2,1)S(1)} %gather_fusion) | copy-start | bytes 1572868 | tf_op jit(solution)/shard_map/while
  172.4 6.1 %copy-start.1 = (bf16[32,64,128]{2,1,0:T(8,128)(2,1)S(1)}, bf16[32,64,128]{2,1,0:T(8,128)(2,1)}, u32[]{:S(2)}) copy-start(bf16[32,64,128]{2,1,0:T(8,128)(2,1)} %copy-done) | copy-start | bytes 1572868 | tf_op jit(solution)/shard_map/while
  186.7 3.6 %copy-start = (bf16[32,64,128]{2,1,0:T(8,128)(2,1)}, bf16[32,64,128]{2,1,0:T(8,128)(2,1)S(1)}, u32[]{:S(2)}) copy-start(bf16[32,64,128]{2,1,0:T(8,128)(2,1)S(1)} %gather_fusion) | copy-start | bytes 1572868 | tf_op jit(solution)/shard_map/while
  191.8 6.0 %copy-start.1 = (bf16[32,64,128]{2,1,0:T(8,128)(2,1)S(1)}, bf16[32,64,128]{2,1,0:T(8,128)(2,1)}, u32[]{:S(2)}) copy-start(bf16[32,64,128]{2,1,0:T(8,128)(2,1)} %copy-done) | copy-start | bytes 1572868 | tf_op jit(solution)/shard_map/while
  203.3 56.2 %all-to-all-start.1 = ((bf16[64,64,2,128]{3,1,2,0:T(8,128)(2,1)}), bf16[64,64,2,128]{3,1,2,0:T(8,128)(2,1)S(1)}, u32[]{:S(2)}, u32[]{:S(2)}) async-start(bf16[64,64,2,128]{3,1,2,0:T(8,128)(2,1)} %slice.48), calls=%async_computation.1 | async-start | bytes 4194304 | tf_op jit(solution)/shard_map/all_to_all | solution.py:122
  266.2 35.0 %all-to-all-start.2 = ((bf16[64,64,128]{2,1,0:T(8,128)(2,1)}), bf16[64,64,128]{2,1,0:T(8,128)(2,1)S(1)}, u32[]{:S(2)}, u32[]{:S(2)}) async-start(bf16[64,64,128]{2,1,0:T(8,128)(2,1)} %bitcast.10), calls=%async_computation.2 | async-start | bytes 2097152 | tf_op jit(solution)/shard_map/all_to_all | solution.py:18
Sparse Core Ops, SparseCore 0:
  30.4 42.7 all-gather.1
where the time goes:
time: 312 us; the launch traced here: 309 us
  waiting for transfers between devices  118 us (38%)
  local copies, waits for them, and re-layouts  63.2 us (20%)
  other arithmetic  45 us (14%)
  starting transfers between devices  26.2 us (8%)
  matrix products  21.7 us (7%)
  loops' own time  20.4 us (7%)
  between operations  14.2 us (5%)
    all_to_all x1, waiting for transfers between devices, local(): lax.all_to_all(outgoing, 'kv', split_axis=0, concat_axis=0, tiled=True)  47.9 us
    all_to_all x1, waiting for transfers between devices, local(): lax.all_to_all(totals[:device_count].astype(jnp.bfloat16), 'kv', split_ax...  42.9 us
    scatter-add x6, other arithmetic, one_block(): totals = totals.at[slot_index, :, group_col, :].add(contribs)  37.4 us
    all_to_all x1, waiting for transfers between devices, sum_at_owner(): lax.all_to_all(pieces, axis, split_axis=0, concat_axis=0, tiled=True)  26.4 us
    another operation x1, loops' own time, local(): lax.scan(one_block, start_totals, jnp.arange(blocks_here, dtype=jnp.int32))  20.4 us
    gather x6, local copies, waits for them, and re-layouts, one_block(): key_table[slot_index, :, group_col, :]  13.9 us
    all_to_all x1, starting transfers between devices, local(): lax.all_to_all(outgoing, 'kv', split_axis=0, concat_axis=0, tiled=True)  13.2 us
    while x1, local copies, waits for them, and re-layouts, local(): lax.scan(one_block, start_totals, jnp.arange(blocks_here, dtype=jnp.int32))  7.08 us
  transfers between devices with their start and end apart: 4, of which 3 were waited for; matrix products, arithmetic and copies ran while one was open for 38% of the time, Pallas kernels for 0%

commit v1 on v0

v1 whole, which is shorter than its diff:
```python
import jax
import jax.numpy as jnp
from jax import lax
from jax.experimental import pallas as pl
from jax.experimental.pallas import tpu as pltpu
from jax.sharding import PartitionSpec as P

HD = 64
BLOCK = 64
GROUPS = 2
PER_GROUP = 4
BLOCKS = 6
LIST = 16
DEVS = 64
COLS = PER_GROUP * BLOCK
CHUNK = 256
LOG2E = 1.4426950408889634
VMEM = pltpu.VMEM
SMEM = pltpu.SMEM


def vmem_spec():
    return pl.BlockSpec(memory_space=VMEM)


def smem_spec():
    return pl.BlockSpec(memory_space=SMEM)


def pack_kernel(sel_ref, keys_ref, values_ref, out_ref, own_ref):
    shape = (BLOCKS * BLOCK, 2 * HD)
    low = lax.broadcasted_iota(jnp.int32, shape, 1) < HD
    keys = keys_ref[...].astype(jnp.float32)
    values = values_ref[...].astype(jnp.float32)
    first = jnp.where(low, keys, pltpu.roll(values, HD, 1)).astype(jnp.bfloat16)
    second = jnp.where(low, pltpu.roll(keys, HD, 1), values).astype(jnp.bfloat16)
    own_ref[0] = first.reshape(BLOCKS, BLOCK, 2 * HD)
    own_ref[1] = second.reshape(BLOCKS, BLOCK, 2 * HD)

    @pl.loop(0, DEVS)
    def _(dest):
        for group in range(GROUPS):
            out_ref[dest, group] = own_ref[group, sel_ref[group, dest]]


def attention_kernel(
    slot_ref,
    near_ref,
    remote_ref,
    own_ref,
    query_ref,
    grad_ref,
    sums_ref,
    sent_ref,
    kept_ref,
    query_grad_ref,
    totals,
    table,
    probs,
    prob_grads,
):
    totals[...] = jnp.zeros_like(totals)
    rows = lax.broadcasted_iota(jnp.int32, (BLOCK, COLS), 0)
    cols = lax.broadcasted_iota(jnp.int32, (BLOCK, COLS), 1)
    behind = rows - lax.rem(cols, BLOCK)
    nt = (((1,), (1,)), ((), ()))
    tn = (((0,), (0,)), ((), ()))
    nn = (((1,), (0,)), ((), ()))

    @pl.loop(0, GROUPS * BLOCKS)
    def _(step):
        group = step // BLOCKS
        position = lax.rem(step, BLOCKS)
        query = query_ref[step]
        grad = grad_ref[step]
        sums = sums_ref[step]
        for entry in range(LIST):
            slot = slot_ref[step, entry]

            @pl.when(slot < DEVS)
            def _():
                table[pl.ds(entry * BLOCK, BLOCK), :] = remote_ref[slot, group]

            @pl.when(slot >= DEVS)
            def _():
                table[pl.ds(entry * BLOCK, BLOCK), :] = own_ref[group, slot - DEVS]

        delta = jnp.zeros((BLOCK, COLS), jnp.float32)
        for entry in range(LIST):
            part = pl.ds(entry * BLOCK, BLOCK)
            pair = table[part, :]
            score = lax.dot_general(pair, query, nt, preferred_element_type=jnp.float32)
            prob_grad = lax.dot_general(pair, grad, nt, preferred_element_type=jnp.float32)
            prob = jnp.exp2(score * (LOG2E * HD**-0.5) - sums)
            prob = jnp.where(behind <= near_ref[step, entry], prob, 0.0)
            delta = delta + prob * prob_grad
            probs[part, :] = prob
            prob_grads[part, :] = prob_grad
        delta = jnp.sum(delta, axis=0, keepdims=True)
        query_grad = jnp.zeros((2 * HD, COLS), jnp.float32)
        for chunk in range(LIST * BLOCK // CHUNK):
            part = pl.ds(chunk * CHUNK, CHUNK)
            prob = probs[part, :]
            score_grad = (prob * (prob_grads[part, :] - delta)).astype(jnp.bfloat16)
            contrib = lax.dot_general(
                score_grad, query, nn, preferred_element_type=jnp.float32
            ) + lax.dot_general(
                prob.astype(jnp.bfloat16), grad, nn, preferred_element_type=jnp.float32
            )
            query_grad = query_grad + lax.dot_general(
                table[part, :], score_grad, tn, preferred_element_type=jnp.float32
            )
            for inner in range(CHUNK // BLOCK):
                entry = chunk * (CHUNK // BLOCK) + inner
                slot = slot_ref[step, entry]
                totals[slot, group] += contrib[inner * BLOCK : (inner + 1) * BLOCK]
        query_grad_ref[step] = query_grad[:HD] * HD**-0.5

    lane = lax.broadcasted_iota(jnp.int32, (BLOCK, 2 * HD), 1)
    factor = jnp.where(lane < HD, HD**-0.5, 1.0)

    @pl.loop(0, DEVS)
    def _(dest):
        for group in range(GROUPS):
            sent_ref[dest, group] = (totals[dest, group] * factor).astype(jnp.bfloat16)

    for block in range(BLOCKS):
        for group in range(GROUPS):
            kept_ref[group, block] = totals[DEVS + block, group] * factor


def collect_kernel(sel_ref, returned_ref, kept_ref, key_ref, value_ref, half_ref, total):
    total[...] = kept_ref[...]

    @pl.loop(0, DEVS)
    def _(source):
        for group in range(GROUPS):
            total[group, sel_ref[group, source]] += returned_ref[source, group].astype(jnp.float32)

    low = lax.broadcasted_iota(jnp.int32, (BLOCKS * BLOCK, 2 * HD), 1) < HD
    first = total[0].reshape(BLOCKS * BLOCK, 2 * HD)
    second = total[1].reshape(BLOCKS * BLOCK, 2 * HD)
    key_grad = jnp.where(low, first, pltpu.roll(second, HD, 1))
    key_ref[...] = key_grad
    half_ref[...] = key_grad.astype(jnp.bfloat16)
    value_ref[...] = jnp.where(low, pltpu.roll(first, HD, 1), second)


def local(queries, key_heads, values, log_sums, out_grad, inputs, chosen):
    me = lax.axis_index("kv")
    rows = BLOCKS * BLOCK
    first = me * BLOCKS
    within = chosen.reshape(GROUPS, DEVS, BLOCKS * LIST) - first
    listed = (within >= 0) & (within < BLOCKS)
    sel = jnp.max(jnp.where(listed, within, 0), axis=2)
    mine = lax.dynamic_slice_in_dim(chosen, first, BLOCKS, 1)
    near = mine - first
    slot = jnp.where(near >= 0, DEVS + near, jnp.maximum(mine, 0) // BLOCKS)
    positions = jnp.arange(BLOCKS, dtype=jnp.int32)[None, :, None]
    near = jnp.where(mine < 0, -BLOCK, jnp.where(near == positions, 0, BLOCK))
    slot = slot.reshape(GROUPS * BLOCKS, LIST)
    near = near.reshape(GROUPS * BLOCKS, LIST)

    bf16 = jnp.bfloat16
    outgoing, own = pl.pallas_call(
        pack_kernel,
        out_shape=(
            jax.ShapeDtypeStruct((DEVS, GROUPS, BLOCK, 2 * HD), bf16),
            jax.ShapeDtypeStruct((GROUPS, BLOCKS, BLOCK, 2 * HD), bf16),
        ),
        in_specs=[smem_spec(), vmem_spec(), vmem_spec()],
        out_specs=(vmem_spec(), vmem_spec()),
        cost_estimate=pl.CostEstimate(flops=1000, bytes_accessed=4 << 20, transcendentals=0),
        name="pack",
    )(sel, key_heads, values)
    remote = lax.all_to_all(outgoing, "kv", split_axis=0, concat_axis=0, tiled=True)
    whole = lax.all_to_all(
        jnp.broadcast_to(inputs[None], (4, *inputs.shape)), "tp", 0, 0, tiled=True
    )

    def by_block(array):
        array = array.reshape(BLOCKS, BLOCK, GROUPS, PER_GROUP, HD)
        return array.transpose(2, 0, 3, 1, 4).reshape(GROUPS * BLOCKS, COLS, HD)

    none = ((0, 0), (0, 0))
    query = jnp.pad(by_block(queries), (*none, (0, HD)))
    grad = jnp.pad(by_block(out_grad), (*none, (HD, 0)))
    sums = log_sums.reshape(GROUPS, PER_GROUP, BLOCKS, BLOCK).transpose(0, 2, 1, 3)
    sums = sums.reshape(GROUPS * BLOCKS, 1, COLS) * LOG2E

    sent, kept, query_grad = pl.pallas_call(
        attention_kernel,
        out_shape=(
            jax.ShapeDtypeStruct((DEVS, GROUPS, BLOCK, 2 * HD), bf16),
            jax.ShapeDtypeStruct((GROUPS, BLOCKS, BLOCK, 2 * HD), jnp.float32),
            jax.ShapeDtypeStruct((GROUPS * BLOCKS, HD, COLS), jnp.float32),
        ),
        in_specs=[smem_spec(), smem_spec(), *[vmem_spec()] * 5],
        out_specs=(vmem_spec(), vmem_spec(), vmem_spec()),
        scratch_shapes=[
            VMEM((DEVS + BLOCKS, GROUPS, BLOCK, 2 * HD), jnp.float32),
            VMEM((LIST * BLOCK, 2 * HD), bf16),
            VMEM((LIST * BLOCK, COLS), jnp.float32),
            VMEM((LIST * BLOCK, COLS), jnp.float32),
        ],
        cost_estimate=pl.CostEstimate(
            flops=4 << 30, bytes_accessed=8 << 20, transcendentals=3 << 20
        ),
        name="attention",
    )(slot, near, remote, own, query, grad, sums)
    returned = lax.all_to_all(sent, "kv", split_axis=0, concat_axis=0, tiled=True)
    query_grad = query_grad.reshape(GROUPS, BLOCKS, HD, PER_GROUP, BLOCK)
    query_grad = query_grad.transpose(1, 4, 0, 3, 2).reshape(rows, GROUPS * PER_GROUP * HD)

    key_grad, value_grad, key_half = pl.pallas_call(
        collect_kernel,
        out_shape=(
            jax.ShapeDtypeStruct((rows, 2 * HD), jnp.float32),
            jax.ShapeDtypeStruct((rows, 2 * HD), jnp.float32),
            jax.ShapeDtypeStruct((rows, 2 * HD), bf16),
        ),
        in_specs=[smem_spec(), vmem_spec(), vmem_spec()],
        out_specs=(vmem_spec(), vmem_spec(), vmem_spec()),
        scratch_shapes=[VMEM((GROUPS, BLOCKS, BLOCK, 2 * HD), jnp.float32)],
        cost_estimate=pl.CostEstimate(flops=2 << 20, bytes_accessed=4 << 20, transcendentals=0),
        name="collect",
    )(sel, returned, kept)
    terms = jnp.einsum("xtf,tc->xfc", whole, key_half, preferred_element_type=jnp.float32)
    terms = terms.astype(bf16).reshape(DEVS, BLOCK, 2 * HD)
    arrived = lax.all_to_all(terms, "kv", split_axis=0, concat_axis=0, tiled=True)
    weight_grad = arrived.astype(jnp.float32).sum(axis=0)
    return (query_grad, key_grad, value_grad, weight_grad)


def solution(mesh):
    placed = (
        P("kv", "tp"),
        P("kv", "tp"),
        P("kv", "tp"),
        P("tp", "kv"),
        P("kv", "tp"),
        P("kv", "tp"),
        P("tp", None, None),
    )
    return jax.shard_map(
        local,
        mesh=mesh,
        in_specs=placed,
        out_specs=(P("kv", "tp"), P("kv", "tp"), P("kv", "tp"), P("kv", "tp")),
        check_vma=False,
    )
```

time: 312 us -> 237 us (0.76)
  blocking collectives: 0 us -> 57 us
  local copies, waits for them, and re-layouts: 63.2 us -> 13.6 us
  other arithmetic: 45 us -> 4.39 us
  Pallas kernels: 0 us -> 31.3 us
  loops' own time: 20.4 us -> 0 us
  matrix products: 21.7 us -> 2.62 us
  waiting for transfers between devices: 118 us -> 99.8 us
  between operations: 14.2 us -> 0.76 us
    all_to_all x0 -> x1, blocking collectives: none -> 57 us  [local(): lax.all_to_all(sent, 'kv', split_axis=0, concat_axis=0, tiled=True)]
    scatter-add x6 -> x0, other arithmetic: 37.4 us -> none  [one_block(): totals = totals.at[slot_index, :, group_col, :].add(contribs)]
    pallas_call x0 -> x3, Pallas kernels: none -> 31.3 us  [the longest x1 25 us: local(): pl.pallas_call(attention_kernel, out_shape=(jax.ShapeDtypeStruct((DEVS, G...]
    another operation x1 -> x0, loops' own time: 20.4 us -> none  [local(): lax.scan(one_block, start_totals, jnp.arange(blocks_here, dtype=jnp.int32))]
    dot_general x33 -> x1, matrix products: 21.7 us -> 2.62 us  [local(): jnp.einsum('xtf,tc->xfc', whole, key_half, preferred_element_type=jnp.flo...]
    dynamic_slice x19 -> x0, local copies, waits for them, and re-layouts: 14.2 us -> none  [the longest x6 5.32 us: one_block(): lax.dynamic_slice_in_dim(out_grad, first_row, BLOCK, 0)]
    gather x6 -> x0, local copies, waits for them, and re-layouts: 13.9 us -> none  [one_block(): key_table[slot_index, :, group_col, :]]
    all_to_all x2, waiting for transfers between devices: 69.3 us -> 56.7 us  [the longest x1 32 us: local(): lax.all_to_all(jnp.broadcast_to(inputs[None], (4, *inputs.shape)), 'tp',...]
  transfers between devices with their start and end apart: 4 -> 3, of which waited for: 3 -> 3; matrix products, arithmetic and copies ran while one was open for 38% -> 4% of each run, Pallas kernels for 0% -> 1%
where the time goes in v1:
time: 237 us; the launch traced here: 236 us
  waiting for transfers between devices  99.8 us (42%)
  blocking collectives  57 us (24%)
  Pallas kernels  31.3 us (13%)
  starting transfers between devices  27 us (11%)
  local copies, waits for them, and re-layouts  13.6 us (6%)
  other arithmetic  4.39 us (2%)
  matrix products  2.62 us (1%)
    all_to_all x1, blocking collectives, local(): lax.all_to_all(sent, 'kv', split_axis=0, concat_axis=0, tiled=True)  57 us
    all_to_all x1, waiting for transfers between devices, local(): lax.all_to_all(outgoing, 'kv', split_axis=0, concat_axis=0, tiled=True)  43.1 us
    all_to_all x1, waiting for transfers between devices, local(): lax.all_to_all(jnp.broadcast_to(inputs[None], (4, *inputs.shape)), 'tp',...  32 us
    pallas_call x1, Pallas kernels, local(): pl.pallas_call(attention_kernel, out_shape=(jax.ShapeDtypeStruct((DEVS, G...  25 us
    all_to_all x1, waiting for transfers between devices, local(): lax.all_to_all(terms, 'kv', split_axis=0, concat_axis=0, tiled=True)  24.7 us
    all_to_all x1, starting transfers between devices, local(): lax.all_to_all(outgoing, 'kv', split_axis=0, concat_axis=0, tiled=True)  13.5 us
    all_to_all x1, starting transfers between devices, local(): lax.all_to_all(terms, 'kv', split_axis=0, concat_axis=0, tiled=True)  9.49 us
  transfers between devices with their start and end apart: 3, of which 3 were waited for; matrix products, arithmetic and copies ran while one was open for 4% of the time, Pallas kernels for 1%

profile of v1, /device:TPU:1, one launch (start us, length us, event | category | flops | bytes accessed | tf_op | source)
XLA Modules:
  0.0 236.3 jit_solution(18036755119185458837)
XLA Ops:
  0.6 0.8 select_reduce_fusion
  1.5 0.1 reduce_max.14
  1.6 0.7 reduce_max.18.sel_ref
  2.3 3.0 %pack.1 = (bf16[64,2,64,128]{3,2,1,0:T(8,128)(2,1)}, bf16[2,6,64,128]{3,2,1,0:T(8,128)(2,1)}) custom-call(s32[2,64]{1,0:T(2,128)} %reduce_max.18.sel_ref, bf16[384,128]{1,0:T(8,128)(2,1)} %keys_ref.1, bf16[384,128]{1,0:T(8,128)(2,1)} %values_ref.1), custom_call_target="tpu_custom_call" | custom-call | flops 1000 | bytes 4194304 | tf_op jit(solution)/shard_map/pack/pallas_call | solution.py:165
  5.3 13.5 %all-to-all-start = ((bf16[64,2,64,128]{3,2,1,0:T(8,128)(2,1)}), bf16[64,2,64,128]{3,2,1,0:T(8,128)(2,1)}, u32[]{:S(2)}, u32[]{:S(2)}) async-start(bf16[64,2,64,128]{3,2,1,0:T(8,128)(2,1)} %get-tuple-element.12), calls=%async_computation | async-start | bytes 4194304 | tf_op jit(solution)/shard_map/all_to_all | solution.py:176
  18.9 0.7 mul.20.sums_ref
  19.6 0.8 select_select_fusion
  20.4 0.1 copy.19
  20.5 0.6 reshape.57.near_ref
  21.1 0.1 copy.18
  21.2 0.6 reshape.56.slot_ref
  21.8 0.4 reshape.58
  22.2 0.2 copy.20
  22.4 0.4 reshape.60
  22.8 0.2 copy.21
  23.0 1.1 pad.8.query_ref
  24.0 1.3 pad.9.grad_ref
  25.3 43.1 %all-to-all-done.remote_ref = bf16[64,2,64,128]{3,2,1,0:T(8,128)(2,1)} async-done(((bf16[64,2,64,128]{3,2,1,0:T(8,128)(2,1)}), bf16[64,2,64,128]{3,2,1,0:T(8,128)(2,1)}, u32[]{:S(2)}, u32[]{:S(2)}) %all-to-all-start) | async-done | bytes 2097184 | tf_op jit(solution)/shard_map/all_to_all | solution.py:176
  68.4 25.0 %attention.1 = (bf16[64,2,64,128]{3,2,1,0:T(8,128)(2,1)}, f32[2,6,64,128]{3,2,1,0:T(8,128)}, f32[12,64,256]{2,1,0:T(8,128)}) custom-call(s32[12,16]{1,0:T(8,128)} %reshape.56.slot_ref, s32[12,16]{1,0:T(8,128)} %reshape.57.near_ref, bf16[64,2,64,128]{3,2,1,0:T(8,128)(2,1)} %all-to-all-done.remote_ref, bf16[2,6,64,128]{3,2,1,0:T(8,128)(2,1)} %get-tuple-element.13.own_ref, ...), custom_call_target="tpu_custom_call" | custom-call | flops 4294967296 | bytes 8388608 | tf_op jit(solution)/shard_map/attention/pallas_call | solution.py:191
  93.4 57.0 %all_to_all.20.returned_ref = bf16[64,2,64,128]{3,2,1,0:T(8,128)(2,1)} all-to-all(bf16[64,2,64,128]{3,2,1,0:T(8,128)(2,1)} %get-tuple-element.15), channel_id=1, replica_groups=mesh['kv'=64,'tp'=4] {'kv'}, dimensions={0} | all-to-all | bytes 4194304 | tf_op jit(solution)/shard_map/all_to_all | solution.py:211
  150.4 2.1 broadcast_in_dim.18
  152.4 4.0 %all-to-all-start.2 = ((bf16[4,384,1024]{2,1,0:T(8,128)(2,1)}), bf16[4,384,1024]{2,1,0:T(8,128)(2,1)S(1)}, u32[]{:S(2)}, u32[]{:S(2)}) async-start(bf16[4,384,1024]{2,1,0:T(8,128)(2,1)} %broadcast_in_dim.18), calls=%async_computation.2 | async-start | bytes 6291456 | tf_op jit(solution)/shard_map/all_to_all | solution.py:177
  156.4 3.3 %collect.1 = (f32[384,128]{1,0:T(8,128)}, f32[384,128]{1,0:T(8,128)}, bf16[384,128]{1,0:T(8,128)(2,1)}) custom-call(s32[2,64]{1,0:T(2,128)} %reduce_max.18.sel_ref, bf16[64,2,64,128]{3,2,1,0:T(8,128)(2,1)} %all_to_all.20.returned_ref, f32[2,6,64,128]{3,2,1,0:T(8,128)} %get-tuple-element.16.kept_ref), custom_call_target="tpu_custom_call" | custom-call | flops 2097152 | bytes 4194304 | tf_op jit(solution)/shard_map/collect/pallas_call | solution.py:215
  159.8 32.0 %all-to-all-done.2 = bf16[4,384,1024]{2,1,0:T(8,128)(2,1)S(1)} async-done(((bf16[4,384,1024]{2,1,0:T(8,128)(2,1)}), bf16[4,384,1024]{2,1,0:T(8,128)(2,1)S(1)}, u32[]{:S(2)}, u32[]{:S(2)}) %all-to-all-start.2) | async-done | bytes 3145760 | tf_op jit(solution)/shard_map/all_to_all | solution.py:177
  191.8 2.6 %fusion = bf16[4,1024,128]{1,2,0:T(8,128)(2,1)} fusion(bf16[4,384,1024]{2,1,0:T(8,128)(2,1)S(1)} %all-to-all-done.2, bf16[384,128]{1,0:T(8,128)(2,1)} %get-tuple-element.19), kind=kOutput, calls=%fused_computation.2 | convolution fusion | flops 403177472 | bytes 4292608 | tf_op jit(solution)/shard_map/xtf,tc->xfc/dot_general | solution.py:228
  194.4 2.3 copy.25
  196.7 9.5 %all-to-all-start.3 = ((bf16[64,64,128]{2,1,0:T(8,128)(2,1)}), bf16[64,64,128]{2,1,0:T(8,128)(2,1)}, u32[]{:S(2)}, u32[]{:S(2)}) async-start(bf16[64,64,128]{2,1,0:T(8,128)(2,1)} %bitcast.8), calls=%async_computation.3 | async-start | bytes 2097152 | tf_op jit(solution)/shard_map/all_to_all | solution.py:230
  206.2 0.7 reshape.62
  206.9 0.9 copy.23
  207.8 1.8 reshape.63
  209.6 24.7 %all-to-all-done.3 = bf16[64,64,128]{2,1,0:T(8,128)(2,1)} async-done(((bf16[64,64,128]{2,1,0:T(8,128)(2,1)}), bf16[64,64,128]{2,1,0:T(8,128)(2,1)}, u32[]{:S(2)}, u32[]{:S(2)}) %all-to-all-start.3) | async-done | bytes 1048608 | tf_op jit(solution)/shard_map/all_to_all | solution.py:230
  234.3 2.0 convert_reduce_fusion
  (13 shorter events, 0.1 us)
Async XLA Ops:
  5.3 13.5 %copy-start.4 = (f32[8,384]{1,0:T(8,128)S(1)}, f32[8,384]{1,0:T(8,128)}, u32[]{:S(2)}) copy-start(f32[8,384]{1,0:T(8,128)} %param.10) | copy-start | bytes 36868
  5.3 16.5 %copy-start.2 = (bf16[384,512]{1,0:T(8,128)(2,1)S(1)}, bf16[384,512]{1,0:T(8,128)(2,1)}, u32[]{:S(2)}) copy-start(bf16[384,512]{1,0:T(8,128)(2,1)} %param.7) | copy-start | bytes 1179652
  5.3 63.1 %all-to-all-start = ((bf16[64,2,64,128]{3,2,1,0:T(8,128)(2,1)}), bf16[64,2,64,128]{3,2,1,0:T(8,128)(2,1)}, u32[]{:S(2)}, u32[]{:S(2)}) async-start(bf16[64,2,64,128]{3,2,1,0:T(8,128)(2,1)} %get-tuple-element.12), calls=%async_computation | async-start | bytes 4194304 | tf_op jit(solution)/shard_map/all_to_all | solution.py:176
  18.8 3.6 %copy-start.3 = (bf16[384,512]{1,0:T(8,128)(2,1)S(1)}, bf16[384,512]{1,0:T(8,128)(2,1)}, u32[]{:S(2)}) copy-start(bf16[384,512]{1,0:T(8,128)(2,1)} %param.11) | copy-start | bytes 1179652
  93.4 57.0 %copy-start.1 = (bf16[384,1024]{1,0:T(8,128)(2,1)S(1)}, bf16[384,1024]{1,0:T(8,128)(2,1)}, u32[]{:S(2)}) copy-start(bf16[384,1024]{1,0:T(8,128)(2,1)} %param.12) | copy-start | bytes 2359300
  152.4 39.4 %all-to-all-start.2 = ((bf16[4,384,1024]{2,1,0:T(8,128)(2,1)}), bf16[4,384,1024]{2,1,0:T(8,128)(2,1)S(1)}, u32[]{:S(2)}, u32[]{:S(2)}) async-start(bf16[4,384,1024]{2,1,0:T(8,128)(2,1)} %broadcast_in_dim.18), calls=%async_computation.2 | async-start | bytes 6291456 | tf_op jit(solution)/shard_map/all_to_all | solution.py:177
  194.4 11.8 %copy-start = (f32[12,64,256]{2,1,0:T(8,128)S(1)}, f32[12,64,256]{2,1,0:T(8,128)}, u32[]{:S(2)}) copy-start(f32[12,64,256]{2,1,0:T(8,128)} %get-tuple-element.14) | copy-start | bytes 2359300
  196.7 37.6 %all-to-all-start.3 = ((bf16[64,64,128]{2,1,0:T(8,128)(2,1)}), bf16[64,64,128]{2,1,0:T(8,128)(2,1)}, u32[]{:S(2)}, u32[]{:S(2)}) async-start(bf16[64,64,128]{2,1,0:T(8,128)(2,1)} %bitcast.8), calls=%async_computation.3 | async-start | bytes 2097152 | tf_op jit(solution)/shard_map/all_to_all | solution.py:230

commit v2 on v1

--- a/solution.py
+++ b/solution.py
@@ -12,6 +12,7 @@
 BLOCKS = 6
 LIST = 16
 DEVS = 64
+TP = 4
 COLS = PER_GROUP * BLOCK
 CHUNK = 256
 LOG2E = 1.4426950408889634
@@ -41,6 +42,10 @@
     def _(dest):
         for group in range(GROUPS):
             out_ref[dest, group] = own_ref[group, sel_ref[group, dest]]
+
+
+def dot(a, b, dims):
+    return lax.dot_general(a, b, (dims, ((), ())), preferred_element_type=jnp.float32)
 
 
 def attention_kernel(
@@ -55,71 +60,78 @@
     kept_ref,
     query_grad_ref,
     totals,
-    table,
-    probs,
-    prob_grads,
+    *scratch,
 ):
     totals[...] = jnp.zeros_like(totals)
     rows = lax.broadcasted_iota(jnp.int32, (BLOCK, COLS), 0)
     cols = lax.broadcasted_iota(jnp.int32, (BLOCK, COLS), 1)
-    behind = rows - lax.rem(cols, BLOCK)
-    nt = (((1,), (1,)), ((), ()))
-    tn = (((0,), (0,)), ((), ()))
-    nn = (((1,), (0,)), ((), ()))
-
-    @pl.loop(0, GROUPS * BLOCKS)
-    def _(step):
+    behind = rows - (cols & (BLOCK - 1))
+    per_chunk = CHUNK // BLOCK
+    even, odd = scratch[:4], scratch[4:]
+
+    def first_pass(step, held, chunk, delta):
+        table, probs, prob_grads, _ = held
         group = step // BLOCKS
-        position = lax.rem(step, BLOCKS)
-        query = query_ref[step]
-        grad = grad_ref[step]
         sums = sums_ref[step]
-        for entry in range(LIST):
+        entries = range(chunk * per_chunk, (chunk + 1) * per_chunk)
+        for entry in entries:
             slot = slot_ref[step, entry]
-
-            @pl.when(slot < DEVS)
-            def _():
-                table[pl.ds(entry * BLOCK, BLOCK), :] = remote_ref[slot, group]
-
-            @pl.when(slot >= DEVS)
-            def _():
-                table[pl.ds(entry * BLOCK, BLOCK), :] = own_ref[group, slot - DEVS]
-
-        delta = jnp.zeros((BLOCK, COLS), jnp.float32)
-        for entry in range(LIST):
-            part = pl.ds(entry * BLOCK, BLOCK)
-            pair = table[part, :]
-            score = lax.dot_general(pair, query, nt, preferred_element_type=jnp.float32)
-            prob_grad = lax.dot_general(pair, grad, nt, preferred_element_type=jnp.float32)
-            prob = jnp.exp2(score * (LOG2E * HD**-0.5) - sums)
+            far = remote_ref[jnp.minimum(slot, DEVS - 1), group]
+            close = own_ref[group, jnp.maximum(slot - DEVS, 0)]
+            table[pl.ds(entry * BLOCK, BLOCK), :] = jnp.where(slot < DEVS, far, close)
+        pair = table[pl.ds(chunk * CHUNK, CHUNK), :]
+        scores = dot(pair, query_ref[step], ((1,), (1,)))
+        grads = dot(pair, grad_ref[step], ((1,), (1,)))
+        for inner, entry in enumerate(entries):
+            part = slice(inner * BLOCK, (inner + 1) * BLOCK)
+            prob = jnp.exp2(scores[part] * (LOG2E * HD**-0.5) - sums)
             prob = jnp.where(behind <= near_ref[step, entry], prob, 0.0)
-            delta = delta + prob * prob_grad
-            probs[part, :] = prob
-            prob_grads[part, :] = prob_grad
-        delta = jnp.sum(delta, axis=0, keepdims=True)
+            delta = delta + jnp.sum((prob * grads[part]).reshape(8, 8, COLS), axis=0)
+            probs[pl.ds(entry * BLOCK, BLOCK), :] = prob
+            prob_grads[pl.ds(entry * BLOCK, BLOCK), :] = grads[part]
+        return delta
+
+    def second_pass(step, held, chunk, query_grad):
+        table, probs, prob_grads, delta = held
+        group = step // BLOCKS
+        part = pl.ds(chunk * CHUNK, CHUNK)
+        prob = probs[part, :]
+        score_grad = (prob * (prob_grads[part, :] - delta[...])).astype(jnp.bfloat16)
+        contrib = dot(score_grad, query_ref[step], ((1,), (0,)))
+        contrib = contrib + dot(prob.astype(jnp.bfloat16), grad_ref[step], ((1,), (0,)))
+        for inner in range(per_chunk):
+            slot = slot_ref[step, chunk * per_chunk + inner]
+            totals[slot, group] += contrib[inner * BLOCK : (inner + 1) * BLOCK]
+        return query_grad + dot(table[part, :], score_grad, ((0,), (0,)))
+
+    def passes(first=None, second=None):
+        delta = jnp.zeros((8, COLS), jnp.float32)
         query_grad = jnp.zeros((2 * HD, COLS), jnp.float32)
         for chunk in range(LIST * BLOCK // CHUNK):
-            part = pl.ds(chunk * CHUNK, CHUNK)
-            prob = probs[part, :]
-            score_grad = (prob * (prob_grads[part, :] - delta)).astype(jnp.bfloat16)
-            contrib = lax.dot_general(
-                score_grad, query, nn, preferred_element_type=jnp.float32
-            ) + lax.dot_general(
-                prob.astype(jnp.bfloat16), grad, nn, preferred_element_type=jnp.float32
-            )
-            query_grad = query_grad + lax.dot_general(
-                table[part, :], score_grad, tn, preferred_element_type=jnp.float32
-            )
-            for inner in range(CHUNK // BLOCK):
-                entry = chunk * (CHUNK // BLOCK) + inner
-                slot = slot_ref[step, entry]
-                totals[slot, group] += contrib[inner * BLOCK : (inner + 1) * BLOCK]
-        query_grad_ref[step] = query_grad[:HD] * HD**-0.5
+            if first is not None:
+                delta = first_pass(*first, chunk, delta)
+            if second is not None:
+                query_grad = second_pass(*second, chunk, query_grad)
+        if first is not None:
+            first[1][3][...] = jnp.sum(delta, axis=0, keepdims=True)
+        if second is not None:
+            query_grad_ref[second[0]] = query_grad[:HD] * HD**-0.5
+
+    last = GROUPS * BLOCKS - 1
+    passes(first=(0, even))
+
+    @pl.loop(0, last // 2)
+    def _(i):
+        passes(first=(2 * i + 1, odd), second=(2 * i, even))
+        passes(first=(2 * i + 2, even), second=(2 * i + 1, odd))
+
+    passes(first=(last, odd), second=(last - 1, even))
+    passes(second=(last, odd))
 
     lane = lax.broadcasted_iota(jnp.int32, (BLOCK, 2 * HD), 1)
     factor = jnp.where(lane < HD, HD**-0.5, 1.0)
 
-    @pl.loop(0, DEVS)
+    @pl.loop(0, DEVS, unroll=4)
     def _(dest):
         for group in range(GROUPS):
             sent_ref[dest, group] = (totals[dest, group] * factor).astype(jnp.bfloat16)
@@ -144,6 +156,13 @@
     key_ref[...] = key_grad
     half_ref[...] = key_grad.astype(jnp.bfloat16)
     value_ref[...] = jnp.where(low, pltpu.roll(first, HD, 1), second)
+
+
+def weight_kernel(tp_ref, key_ref, *refs):
+    *pieces, out_ref = refs
+    for shift, piece in enumerate(pieces):
+        terms = dot(piece[...], key_ref[...], ((1,), (0,)))
+        out_ref[lax.rem(tp_ref[0] + TP - shift, TP)] = terms.astype(jnp.bfloat16)
 
 
 def local(queries, key_heads, values, log_sums, out_grad, inputs, chosen):
@@ -174,9 +193,18 @@
         name="pack",
     )(sel, key_heads, values)
     remote = lax.all_to_all(outgoing, "kv", split_axis=0, concat_axis=0, tiled=True)
-    whole = lax.all_to_all(
-        jnp.broadcast_to(inputs[None], (4, *inputs.shape)), "tp", 0, 0, tiled=True
+    core = me % 2
+    halves = inputs.reshape(rows, 8, 2, HD)
+    mine, theirs = (
+        jnp.where(core == parity, halves[:, :, 0], halves[:, :, 1]).reshape(rows, 8 * HD)
+        for parity in range(2)
     )
+    partner = [(i, i ^ 1) for i in range(DEVS)]
+    features = jnp.concatenate([mine, lax.ppermute(theirs, "kv", partner)], axis=0).T
+    pieces = [features]
+    for shift in range(1, TP):
+        ring = [(i, (i + shift) % TP) for i in range(TP)]
+        pieces.append(lax.ppermute(features, "tp", ring))
 
     def by_block(array):
         array = array.reshape(BLOCKS, BLOCK, GROUPS, PER_GROUP, HD)
@@ -188,6 +216,12 @@
     sums = log_sums.reshape(GROUPS, PER_GROUP, BLOCKS, BLOCK).transpose(0, 2, 1, 3)
     sums = sums.reshape(GROUPS * BLOCKS, 1, COLS) * LOG2E
 
+    held = [
+        VMEM((LIST * BLOCK, 2 * HD), bf16),
+        VMEM((LIST * BLOCK, COLS), jnp.float32),
+        VMEM((LIST * BLOCK, COLS), jnp.float32),
+        VMEM((1, COLS), jnp.float32),
+    ]
     sent, kept, query_grad = pl.pallas_call(
         attention_kernel,
         out_shape=(
@@ -199,9 +233,8 @@
         out_specs=(vmem_spec(), vmem_spec(), vmem_spec()),
         scratch_shapes=[
             VMEM((DEVS + BLOCKS, GROUPS, BLOCK, 2 * HD), jnp.float32),
-            VMEM((LIST * BLOCK, 2 * HD), bf16),
-            VMEM((LIST * BLOCK, COLS), jnp.float32),
-            VMEM((LIST * BLOCK, COLS), jnp.float32),
+            *held,
+            *held,
         ],
         cost_estimate=pl.CostEstimate(
             flops=4 << 30, bytes_accessed=8 << 20, transcendentals=3 << 20
@@ -225,9 +258,18 @@
         cost_estimate=pl.CostEstimate(flops=2 << 20, bytes_accessed=4 << 20, transcendentals=0),
         name="collect",
     )(sel, returned, kept)
-    terms = jnp.einsum("xtf,tc->xfc", whole, key_half, preferred_element_type=jnp.float32)
-    terms = terms.astype(bf16).reshape(DEVS, BLOCK, 2 * HD)
-    arrived = lax.all_to_all(terms, "kv", split_axis=0, concat_axis=0, tiled=True)
+    key_pair = jnp.concatenate([key_half, lax.ppermute(key_half, "kv", partner)], axis=0)
+    terms = pl.pallas_call(
+        weight_kernel,
+        out_shape=jax.ShapeDtypeStruct((TP, 8 * HD, 2 * HD), bf16),
+        in_specs=[smem_spec(), *[vmem_spec()] * 5],
+        out_specs=vmem_spec(),
+        cost_estimate=pl.CostEstimate(flops=1 << 29, bytes_accessed=4 << 20, transcendentals=0),
+        name="weights",
+    )(lax.axis_index("tp").reshape(1), key_pair, *pieces)
+    same_core = [list(range(parity, DEVS, 2)) for parity in range(2)]
+    terms = terms.reshape(DEVS // 2, HD, 2 * HD)
+    arrived = lax.all_to_all(terms, "kv", 0, 0, tiled=True, axis_index_groups=same_core)
     weight_grad = arrived.astype(jnp.float32).sum(axis=0)
     return (query_grad, key_grad, value_grad, weight_grad)
 

time: 237 us -> 176 us (0.74)
  blocking collectives: 57 us -> 0 us
  Pallas kernels: 31.3 us -> 23.7 us
  starting transfers between devices: 27 us -> 32.9 us
  matrix products: 2.62 us -> 0 us
    all_to_all x1 -> x0, blocking collectives: 57 us -> none  [local(): lax.all_to_all(sent, 'kv', split_axis=0, concat_axis=0, tiled=True)]
    pallas_call x1, Pallas kernels: 25 us -> 13.8 us  [local(): pl.pallas_call(attention_kernel, out_shape=(jax.ShapeDtypeStruct((DEVS, G...]
    ppermute x0 -> x5, starting transfers between devices: none -> 7.51 us  [the longest x3 4.89 us: local(): pieces.append(lax.ppermute(features, 'tp', ring))]
    pallas_call x0 -> x1, Pallas kernels: none -> 3.68 us  [local(): pl.pallas_call(weight_kernel, out_shape=jax.ShapeDtypeStruct((TP, 8 * HD,...]
    unnamed x10 -> x13, local copies, waits for them, and re-layouts: 0.02 us -> 2.84 us
    dot_general x1 -> x0, matrix products: 2.62 us -> none  [local(): jnp.einsum('xtf,tc->xfc', whole, key_half, preferred_element_type=jnp.flo...]
    ppermute x0 -> x5, waiting for transfers between devices: none -> 2.51 us  [the longest x1 1.35 us: local(): lax.ppermute(theirs, 'kv', partner)]
  transfers between devices with their start and end apart: 3 -> 8, of which waited for: 3 -> 5; matrix products, arithmetic and copies ran while one was open for 4% -> 7% of each run, Pallas kernels for 1% -> 2%
where the time goes in v2:
time: 176 us; the launch traced here: 175 us
  waiting for transfers between devices  100 us (57%)
  starting transfers between devices  32.9 us (19%)
  Pallas kernels  23.7 us (13%)
  local copies, waits for them, and re-layouts  12 us (7%)
  other arithmetic  5.86 us (3%)
    all_to_all x1, waiting for transfers between devices, local(): lax.all_to_all(outgoing, 'kv', split_axis=0, concat_axis=0, tiled=True)  43 us
    all_to_all x1, waiting for transfers between devices, local(): lax.all_to_all(sent, 'kv', split_axis=0, concat_axis=0, tiled=True)  41.2 us
    pallas_call x1, Pallas kernels, local(): pl.pallas_call(attention_kernel, out_shape=(jax.ShapeDtypeStruct((DEVS, G...  13.8 us
    all_to_all x1, starting transfers between devices, local(): lax.all_to_all(outgoing, 'kv', split_axis=0, concat_axis=0, tiled=True)  13.5 us
    all_to_all x1, waiting for transfers between devices, local(): lax.all_to_all(terms, 'kv', 0, 0, tiled=True, axis_index_groups=same_core)  13.3 us
    all_to_all x1, starting transfers between devices, local(): lax.all_to_all(sent, 'kv', split_axis=0, concat_axis=0, tiled=True)  6.96 us
    all_to_all x1, starting transfers between devices, local(): lax.all_to_all(terms, 'kv', 0, 0, tiled=True, axis_index_groups=same_core)  4.94 us
    ppermute x3, starting transfers between devices, local(): pieces.append(lax.ppermute(features, 'tp', ring))  4.89 us
  transfers between devices with their start and end apart: 8, of which 5 were waited for; matrix products, arithmetic and copies ran while one was open for 7% of the time, Pallas kernels for 2%

profile of v2, /device:TPU:1, one launch (start us, length us, event | category | flops | bytes accessed | tf_op | source)
XLA Modules:
  0.0 175.3 jit_solution(14417784712379827629)
XLA Ops:
  0.6 0.8 select_reduce_fusion
  1.6 0.7 reduce_max.18.sel_ref
  2.3 3.0 %pack.1 = (bf16[64,2,64,128]{3,2,1,0:T(8,128)(2,1)}, bf16[2,6,64,128]{3,2,1,0:T(8,128)(2,1)}) custom-call(s32[2,64]{1,0:T(2,128)} %reduce_max.18.sel_ref, bf16[384,128]{1,0:T(8,128)(2,1)} %keys_ref.1, bf16[384,128]{1,0:T(8,128)(2,1)} %values_ref.1), custom_call_target="tpu_custom_call" | custom-call | flops 1000 | bytes 4194304 | tf_op jit(solution)/shard_map/pack/pallas_call | solution.py:184
  5.2 13.5 %all-to-all-start = ((bf16[64,2,64,128]{3,2,1,0:T(8,128)(2,1)}), bf16[64,2,64,128]{3,2,1,0:T(8,128)(2,1)}, u32[]{:S(2)}, u32[]{:S(2)}) async-start(bf16[64,2,64,128]{3,2,1,0:T(8,128)(2,1)} %get-tuple-element.12), calls=%async_computation | async-start | bytes 4194304 | tf_op jit(solution)/shard_map/all_to_all | solution.py:195
  18.7 0.9 select_select_fusion
  19.7 0.6 reshape.71.slot_ref
  20.4 0.6 reshape.72.near_ref
  22.2 1.1 pad.8.query_ref
  23.3 1.2 pad.9.grad_ref
  24.6 0.7 mul.20.sums_ref
  25.3 43.0 %all-to-all-done.remote_ref = bf16[64,2,64,128]{3,2,1,0:T(8,128)(2,1)} async-done(((bf16[64,2,64,128]{3,2,1,0:T(8,128)(2,1)}), bf16[64,2,64,128]{3,2,1,0:T(8,128)(2,1)}, u32[]{:S(2)}, u32[]{:S(2)}) %all-to-all-start) | async-done | bytes 2097184 | tf_op jit(solution)/shard_map/all_to_all | solution.py:195
  68.3 13.8 %attention.1 = (bf16[64,2,64,128]{3,2,1,0:T(8,128)(2,1)}, f32[2,6,64,128]{3,2,1,0:T(8,128)}, f32[12,64,256]{2,1,0:T(8,128)}) custom-call(s32[12,16]{1,0:T(8,128)} %reshape.71.slot_ref, s32[12,16]{1,0:T(8,128)} %reshape.72.near_ref, bf16[64,2,64,128]{3,2,1,0:T(8,128)(2,1)} %all-to-all-done.remote_ref, bf16[2,6,64,128]{3,2,1,0:T(8,128)(2,1)} %get-tuple-element.13.own_ref, ...), custom_call_target="tpu_custom_call" | custom-call | flops 4294967296 | bytes 8388608 | tf_op jit(solution)/shard_map/attention/pallas_call | solution.py:225
  82.1 7.0 %all-to-all-start.1 = ((bf16[64,2,64,128]{3,2,1,0:T(8,128)(2,1)}), bf16[64,2,64,128]{3,2,1,0:T(8,128)(2,1)S(1)}, u32[]{:S(2)}, u32[]{:S(2)}) async-start(bf16[64,2,64,128]{3,2,1,0:T(8,128)(2,1)} %get-tuple-element.15), calls=%async_computation.1 | async-start | bytes 4194304 | tf_op jit(solution)/shard_map/all_to_all | solution.py:244
  89.1 1.5 copy.25
  90.7 0.5 collective-permute-start.1
  91.2 1.3 collective-permute-done.1
  92.6 1.3 collective-permute-start.2
  93.9 2.5 %collective-permute-start.3 = (bf16[512,768]{1,0:T(8,128)(2,1)S(1)}, bf16[512,768]{1,0:T(8,128)(2,1)}, u32[]{:S(2)}, u32[]{:S(2)}) collective-permute-start(bf16[512,768]{1,0:T(8,128)(2,1)S(1)} %maximum_bitcast_fusion.refs_0_), channel_id=1, source_target_pairs={{0,2},{1,3},{2,0},{3,1},{4,6},{5,7},{6,4},{7,5},{8,10},{9,11},{10,... | collective-permute-start | bytes 2359304 | tf_op jit(solution)/shard_map/ppermute | solution.py:207
  96.4 1.1 collective-permute-start.4
  97.5 41.2 %all-to-all-done.1.returned_ref = bf16[64,2,64,128]{3,2,1,0:T(8,128)(2,1)S(1)} async-done(((bf16[64,2,64,128]{3,2,1,0:T(8,128)(2,1)}), bf16[64,2,64,128]{3,2,1,0:T(8,128)(2,1)S(1)}, u32[]{:S(2)}, u32[]{:S(2)}) %all-to-all-start.1) | async-done | bytes 2097184 | tf_op jit(solution)/shard_map/all_to_all | solution.py:244
  138.8 1.3 copy-done
  140.1 3.3 %collect.1 = (f32[384,128]{1,0:T(8,128)}, f32[384,128]{1,0:T(8,128)}, bf16[384,128]{1,0:T(8,128)(2,1)}) custom-call(s32[2,64]{1,0:T(2,128)} %reduce_max.18.sel_ref, bf16[64,2,64,128]{3,2,1,0:T(8,128)(2,1)} %copy-done, f32[2,6,64,128]{3,2,1,0:T(8,128)} %get-tuple-element.16.kept_ref), custom_call_target="tpu_custom_call" | custom-call | flops 2097152 | bytes 4194304 | tf_op jit(solution)/shard_map/collect/pallas_call | solution.py:248
  143.4 2.1 %collective-permute-start = (bf16[384,128]{1,0:T(8,128)(2,1)}, bf16[384,128]{1,0:T(8,128)(2,1)S(1)}, u32[]{:S(2)}, u32[]{:S(2)}) collective-permute-start(bf16[384,128]{1,0:T(8,128)(2,1)} %get-tuple-element.19), channel_id=1, source_target_pairs={{0,4},{4,0},{8,12},{12,8},{16,20},{20,16},{24,28},{28,24},{32,36},... | collective-permute-start | bytes 294920 | tf_op jit(solution)/shard_map/ppermute | solution.py:261
  145.5 1.2 collective-permute-done
  146.6 1.6 pad_maximum_fusion.key_ref
  148.3 3.7 %weights.1 = bf16[4,512,128]{2,1,0:T(8,128)(2,1)} custom-call(s32[1]{0:T(128)} %bitcast.6.tp_ref, bf16[768,128]{1,0:T(8,128)(2,1)} %pad_maximum_fusion.key_ref, bf16[512,768]{1,0:T(8,128)(2,1)} %copy-done.1, bf16[512,768]{1,0:T(8,128)(2,1)} %collective-permute-done.2.refs_1_, bf16[512,768]{1,0:T(8,128)(2,1)} %collective-permute-done.3.refs_2_, ...), custom_call_target="tpu_custom_call" | custom-call | flops 536870912 | bytes 4194304 | tf_op jit(solution)/shard_map/weights/pallas_call | solution.py:262
  151.9 4.9 %all-to-all-start.2 = ((bf16[32,64,128]{2,1,0:T(8,128)(2,1)}), bf16[32,64,128]{2,1,0:T(8,128)(2,1)}, u32[]{:S(2)}, u32[]{:S(2)}) async-start(bf16[32,64,128]{2,1,0:T(8,128)(2,1)} %bitcast.19), calls=%async_computation.2 | async-start | bytes 1048576 | tf_op jit(solution)/shard_map/all_to_all | solution.py:272
  156.9 0.7 reshape.77
  157.6 0.9 copy.24
  158.4 1.8 %reshape.78 = f32[384,512]{1,0:T(8,128)} reshape(f32[6,64,2,4,64]{4,3,2,1,0:T(4,128)S(1)} %copy.24) | data formatting | bytes 1572864 | tf_op jit(solution)/shard_map/reshape | solution.py:246
  160.3 13.3 %all-to-all-done.2 = bf16[32,64,128]{2,1,0:T(8,128)(2,1)} async-done(((bf16[32,64,128]{2,1,0:T(8,128)(2,1)}), bf16[32,64,128]{2,1,0:T(8,128)(2,1)}, u32[]{:S(2)}, u32[]{:S(2)}) %all-to-all-start.2) | async-done | bytes 524320 | tf_op jit(solution)/shard_map/all_to_all | solution.py:272
  173.6 1.7 convert_reduce_fusion
  (26 shorter events, 1.7 us)
Async XLA Ops:
  5.2 15.8 %copy-start.3 = (bf16[384,512]{1,0:T(8,128)(2,1)S(1)}, bf16[384,512]{1,0:T(8,128)(2,1)}, u32[]{:S(2)}) copy-start(bf16[384,512]{1,0:T(8,128)(2,1)} %param.7) | copy-start | bytes 1179652
  5.2 63.1 %all-to-all-start = ((bf16[64,2,64,128]{3,2,1,0:T(8,128)(2,1)}), bf16[64,2,64,128]{3,2,1,0:T(8,128)(2,1)}, u32[]{:S(2)}, u32[]{:S(2)}) async-start(bf16[64,2,64,128]{3,2,1,0:T(8,128)(2,1)} %get-tuple-element.12), calls=%async_computation | async-start | bytes 4194304 | tf_op jit(solution)/shard_map/all_to_all | solution.py:195
  18.7 2.9 %copy-start.4 = (bf16[384,512]{1,0:T(8,128)(2,1)S(1)}, bf16[384,512]{1,0:T(8,128)(2,1)}, u32[]{:S(2)}) copy-start(bf16[384,512]{1,0:T(8,128)(2,1)} %param.11) | copy-start | bytes 1179652
  22.2 2.3 %copy-start.5 = (f32[8,384]{1,0:T(8,128)S(1)}, f32[8,384]{1,0:T(8,128)}, u32[]{:S(2)}) copy-start(f32[8,384]{1,0:T(8,128)} %param.10) | copy-start | bytes 36868
  82.1 56.7 %all-to-all-start.1 = ((bf16[64,2,64,128]{3,2,1,0:T(8,128)(2,1)}), bf16[64,2,64,128]{3,2,1,0:T(8,128)(2,1)S(1)}, u32[]{:S(2)}, u32[]{:S(2)}) async-start(bf16[64,2,64,128]{3,2,1,0:T(8,128)(2,1)} %get-tuple-element.15), calls=%async_computation.1 | async-start | bytes 4194304 | tf_op jit(solution)/shard_map/all_to_all | solution.py:244
  90.7 1.9 %collective-permute-start.1 = (bf16[384,512]{0,1:T(8,128)(2,1)S(1)}, bf16[384,512]{0,1:T(8,128)(2,1)S(1)}, u32[]{:S(2)}, u32[]{:S(2)}) collective-permute-start(bf16[384,512]{0,1:T(8,128)(2,1)S(1)} %bitcast.21), channel_id=1, source_target_pairs={{0,4},{4,0},{8,12},{12,8},{16,20},{20,16},{24,28},{28,24},{32,36},... | collective-permute-start | bytes 1179656 | tf_op jit(solution)/shard_map/ppermute | solution.py:203
  92.6 55.6 %copy-start.1 = (bf16[512,768]{1,0:T(8,128)(2,1)}, bf16[512,768]{1,0:T(8,128)(2,1)S(1)}, u32[]{:S(2)}) copy-start(bf16[512,768]{1,0:T(8,128)(2,1)S(1)} %maximum_bitcast_fusion.refs_0_) | copy-start | bytes 2359300
  92.6 55.6 %collective-permute-start.2 = (bf16[512,768]{1,0:T(8,128)(2,1)S(1)}, bf16[512,768]{1,0:T(8,128)(2,1)}, u32[]{:S(2)}, u32[]{:S(2)}) collective-permute-start(bf16[512,768]{1,0:T(8,128)(2,1)S(1)} %maximum_bitcast_fusion.refs_0_), channel_id=1, source_target_pairs={{0,1},{1,2},{2,3},{3,0},{4,5},{5,6},{6,7},{7,4},{8,9},{9,10},{10,1... | collective-permute-start | bytes 2359304 | tf_op jit(solution)/shard_map/ppermute | solution.py:207
  93.9 54.3 %collective-permute-start.3 = (bf16[512,768]{1,0:T(8,128)(2,1)S(1)}, bf16[512,768]{1,0:T(8,128)(2,1)}, u32[]{:S(2)}, u32[]{:S(2)}) collective-permute-start(bf16[512,768]{1,0:T(8,128)(2,1)S(1)} %maximum_bitcast_fusion.refs_0_), channel_id=1, source_target_pairs={{0,2},{1,3},{2,0},{3,1},{4,6},{5,7},{6,4},{7,5},{8,10},{9,11},{10,... | collective-permute-start | bytes 2359304 | tf_op jit(solution)/shard_map/ppermute | solution.py:207
  96.4 51.9 %collective-permute-start.4 = (bf16[512,768]{1,0:T(8,128)(2,1)S(1)}, bf16[512,768]{1,0:T(8,128)(2,1)}, u32[]{:S(2)}, u32[]{:S(2)}) collective-permute-start(bf16[512,768]{1,0:T(8,128)(2,1)S(1)} %maximum_bitcast_fusion.refs_0_), channel_id=1, source_target_pairs={{0,3},{1,0},{2,1},{3,2},{4,7},{5,4},{6,5},{7,6},{8,11},{9,8},{10,9... | collective-permute-start | bytes 2359304 | tf_op jit(solution)/shard_map/ppermute | solution.py:207
  138.8 1.3 copy-start
  143.4 3.2 %collective-permute-start = (bf16[384,128]{1,0:T(8,128)(2,1)}, bf16[384,128]{1,0:T(8,128)(2,1)S(1)}, u32[]{:S(2)}, u32[]{:S(2)}) collective-permute-start(bf16[384,128]{1,0:T(8,128)(2,1)} %get-tuple-element.19), channel_id=1, source_target_pairs={{0,4},{4,0},{8,12},{12,8},{16,20},{20,16},{24,28},{28,24},{32,36},... | collective-permute-start | bytes 294920 | tf_op jit(solution)/shard_map/ppermute | solution.py:261
  151.9 4.9 %copy-start.2 = (f32[12,64,256]{2,1,0:T(8,128)S(1)}, f32[12,64,256]{2,1,0:T(8,128)}, u32[]{:S(2)}) copy-start(f32[12,64,256]{2,1,0:T(8,128)} %get-tuple-element.14) | copy-start | bytes 2359300
  151.9 21.6 %all-to-all-start.2 = ((bf16[32,64,128]{2,1,0:T(8,128)(2,1)}), bf16[32,64,128]{2,1,0:T(8,128)(2,1)}, u32[]{:S(2)}, u32[]{:S(2)}) async-start(bf16[32,64,128]{2,1,0:T(8,128)(2,1)} %bitcast.19), calls=%async_computation.2 | async-start | bytes 1048576 | tf_op jit(solution)/shard_map/all_to_all | solution.py:272

commit v3 on v2

--- a/solution.py
+++ b/solution.py
@@ -14,7 +14,9 @@
 DEVS = 64
 TP = 4
 COLS = PER_GROUP * BLOCK
-CHUNK = 256
+CHUNK = 1024
+PACKED = 16
+STREAMS = 8
 LOG2E = 1.4426950408889634
 VMEM = pltpu.VMEM
 SMEM = pltpu.SMEM
@@ -24,24 +26,29 @@
     return pl.BlockSpec(memory_space=VMEM)
 
 
+def any_spec():
+    return pl.BlockSpec(memory_space=pl.ANY)
+
+
 def smem_spec():
     return pl.BlockSpec(memory_space=SMEM)
 
 
 def pack_kernel(sel_ref, keys_ref, values_ref, out_ref, own_ref):
-    shape = (BLOCKS * BLOCK, 2 * HD)
-    low = lax.broadcasted_iota(jnp.int32, shape, 1) < HD
-    keys = keys_ref[...].astype(jnp.float32)
-    values = values_ref[...].astype(jnp.float32)
-    first = jnp.where(low, keys, pltpu.roll(values, HD, 1)).astype(jnp.bfloat16)
-    second = jnp.where(low, pltpu.roll(keys, HD, 1), values).astype(jnp.bfloat16)
-    own_ref[0] = first.reshape(BLOCKS, BLOCK, 2 * HD)
-    own_ref[1] = second.reshape(BLOCKS, BLOCK, 2 * HD)
-
-    @pl.loop(0, DEVS)
-    def _(dest):
+    @pl.when(pl.program_id(0) == 0)
+    def _():
+        low = lax.broadcasted_iota(jnp.int32, (BLOCKS * BLOCK, 2 * HD), 1) < HD
+        keys = keys_ref[...].astype(jnp.float32)
+        values = values_ref[...].astype(jnp.float32)
+        first = jnp.where(low, keys, pltpu.roll(values, HD, 1)).astype(jnp.bfloat16)
+        second = jnp.where(low, pltpu.roll(keys, HD, 1), values).astype(jnp.bfloat16)
+        own_ref[0] = first.reshape(BLOCKS, BLOCK, 2 * HD)
+        own_ref[1] = second.reshape(BLOCKS, BLOCK, 2 * HD)
+
+    for inner in range(PACKED):
+        dest = pl.program_id(0) * PACKED + inner
         for group in range(GROUPS):
-            out_ref[dest, group] = own_ref[group, sel_ref[group, dest]]
+            out_ref[inner, group] = own_ref[group, sel_ref[group, dest]]
 
 
 def dot(a, b, dims):
@@ -102,11 +109,11 @@
         for inner in range(per_chunk):
             slot = slot_ref[step, chunk * per_chunk + inner]
             totals[slot, group] += contrib[inner * BLOCK : (inner + 1) * BLOCK]
-        return query_grad + dot(table[part, :], score_grad, ((0,), (0,)))
+        return query_grad + dot(table[part, :HD], score_grad, ((0,), (0,)))
 
     def passes(first=None, second=None):
         delta = jnp.zeros((8, COLS), jnp.float32)
-        query_grad = jnp.zeros((2 * HD, COLS), jnp.float32)
+        query_grad = jnp.zeros((HD, COLS), jnp.float32)
         for chunk in range(LIST * BLOCK // CHUNK):
             if first is not None:
                 delta = first_pass(*first, chunk, delta)
@@ -115,7 +122,7 @@
         if first is not None:
             first[1][3][...] = jnp.sum(delta, axis=0, keepdims=True)
         if second is not None:
-            query_grad_ref[second[0]] = query_grad[:HD] * HD**-0.5
+            query_grad_ref[second[0]] = query_grad * HD**-0.5
 
     last = GROUPS * BLOCKS - 1
     passes(first=(0, even))
@@ -141,13 +148,27 @@
             kept_ref[group, block] = totals[DEVS + block, group] * factor
 
 
-def collect_kernel(sel_ref, returned_ref, kept_ref, key_ref, value_ref, half_ref, total):
+def collect_kernel(
+    sel_ref, returned_any, kept_ref, key_ref, value_ref, half_ref, total, returned, sems
+):
+    peers = DEVS // STREAMS
+    copies = [
+        pltpu.make_async_copy(
+            returned_any.at[pl.ds(stream * peers, peers)],
+            returned.at[pl.ds(stream * peers, peers)],
+            sems.at[stream],
+        )
+        for stream in range(STREAMS)
+    ]
+    for copy in copies:
+        copy.start()
     total[...] = kept_ref[...]
-
-    @pl.loop(0, DEVS)
-    def _(source):
-        for group in range(GROUPS):
-            total[group, sel_ref[group, source]] += returned_ref[source, group].astype(jnp.float32)
+    for stream, copy in enumerate(copies):
+        copy.wait()
+        for source in range(stream * peers, (stream + 1) * peers):
+            for group in range(GROUPS):
+                block = sel_ref[group, source]
+                total[group, block] += returned[source, group].astype(jnp.float32)
 
     low = lax.broadcasted_iota(jnp.int32, (BLOCKS * BLOCK, 2 * HD), 1) < HD
     first = total[0].reshape(BLOCKS * BLOCK, 2 * HD)
@@ -158,10 +179,19 @@
     value_ref[...] = jnp.where(low, pltpu.roll(first, HD, 1), second)
 
 
-def weight_kernel(tp_ref, key_ref, *refs):
-    *pieces, out_ref = refs
-    for shift, piece in enumerate(pieces):
-        terms = dot(piece[...], key_ref[...], ((1,), (0,)))
+def weight_kernel(tp_ref, near_ref, far_ref, *refs):
+    pieces, (out_ref, held, sems) = refs[:TP], refs[TP:]
+    rows = BLOCKS * BLOCK
+    copies = [
+        pltpu.make_async_copy(piece, held.at[shift], sems.at[shift])
+        for shift, piece in enumerate(pieces)
+    ]
+    for copy in copies:
+        copy.start()
+    for shift, copy in enumerate(copies):
+        copy.wait()
+        terms = dot(held[shift, :, :rows], near_ref[...], ((1,), (0,)))
+        terms = terms + dot(held[shift, :, rows:], far_ref[...], ((1,), (0,)))
         out_ref[lax.rem(tp_ref[0] + TP - shift, TP)] = terms.astype(jnp.bfloat16)
 
 
@@ -187,8 +217,16 @@
             jax.ShapeDtypeStruct((DEVS, GROUPS, BLOCK, 2 * HD), bf16),
             jax.ShapeDtypeStruct((GROUPS, BLOCKS, BLOCK, 2 * HD), bf16),
         ),
-        in_specs=[smem_spec(), vmem_spec(), vmem_spec()],
-        out_specs=(vmem_spec(), vmem_spec()),
+        grid=(DEVS // PACKED,),
+        in_specs=[
+            smem_spec(),
+            pl.BlockSpec((rows, 2 * HD), lambda i: (0, 0)),
+            pl.BlockSpec((rows, 2 * HD), lambda i: (0, 0)),
+        ],
+        out_specs=(
+            pl.BlockSpec((PACKED, GROUPS, BLOCK, 2 * HD), lambda i: (i, 0, 0, 0)),
+            pl.BlockSpec((GROUPS, BLOCKS, BLOCK, 2 * HD), lambda i: (0, 0, 0, 0)),
+        ),
         cost_estimate=pl.CostEstimate(flops=1000, bytes_accessed=4 << 20, transcendentals=0),
         name="pack",
     )(sel, key_heads, values)
@@ -252,21 +290,31 @@
             jax.ShapeDtypeStruct((rows, 2 * HD), jnp.float32),
             jax.ShapeDtypeStruct((rows, 2 * HD), bf16),
         ),
-        in_specs=[smem_spec(), vmem_spec(), vmem_spec()],
+        in_specs=[smem_spec(), any_spec(), vmem_spec()],
         out_specs=(vmem_spec(), vmem_spec(), vmem_spec()),
-        scratch_shapes=[VMEM((GROUPS, BLOCKS, BLOCK, 2 * HD), jnp.float32)],
+        scratch_shapes=[
+            VMEM((GROUPS, BLOCKS, BLOCK, 2 * HD), jnp.float32),
+            VMEM((DEVS, GROUPS, BLOCK, 2 * HD), bf16),
+            pltpu.SemaphoreType.DMA((STREAMS,)),
+        ],
+        compiler_params=pltpu.CompilerParams(vmem_limit_bytes=24 << 20),
         cost_estimate=pl.CostEstimate(flops=2 << 20, bytes_accessed=4 << 20, transcendentals=0),
         name="collect",
     )(sel, returned, kept)
-    key_pair = jnp.concatenate([key_half, lax.ppermute(key_half, "kv", partner)], axis=0)
+    key_far = lax.ppermute(key_half, "kv", partner)
     terms = pl.pallas_call(
         weight_kernel,
         out_shape=jax.ShapeDtypeStruct((TP, 8 * HD, 2 * HD), bf16),
-        in_specs=[smem_spec(), *[vmem_spec()] * 5],
+        in_specs=[smem_spec(), vmem_spec(), vmem_spec(), *[any_spec()] * TP],
         out_specs=vmem_spec(),
+        scratch_shapes=[
+            VMEM((TP, 8 * HD, 2 * rows), bf16),
+            pltpu.SemaphoreType.DMA((TP,)),
+        ],
+        compiler_params=pltpu.CompilerParams(vmem_limit_bytes=24 << 20),
         cost_estimate=pl.CostEstimate(flops=1 << 29, bytes_accessed=4 << 20, transcendentals=0),
         name="weights",
-    )(lax.axis_index("tp").reshape(1), key_pair, *pieces)
+    )(lax.axis_index("tp").reshape(1), key_half, key_far, *pieces)
     same_core = [list(range(parity, DEVS, 2)) for parity in range(2)]
     terms = terms.reshape(DEVS // 2, HD, 2 * HD)
     arrived = lax.all_to_all(terms, "kv", 0, 0, tiled=True, axis_index_groups=same_core)

time: 176 us -> 172 us (0.977)
  transfers between devices with their start and end apart: 8 -> 8, of which waited for: 5 -> 5; matrix products, arithmetic and copies ran while one was open for 7% -> 7% of each run, Pallas kernels for 2% -> 1%
where the time goes in v3:
time: 172 us; the launch traced here: 170 us
  waiting for transfers between devices  99.7 us (58%)
  starting transfers between devices  33 us (19%)
  Pallas kernels  22 us (13%)
  local copies, waits for them, and re-layouts  10.6 us (6%)
  other arithmetic  4.28 us (2%)
    all_to_all x1, waiting for transfers between devices, local(): lax.all_to_all(outgoing, 'kv', split_axis=0, concat_axis=0, tiled=True)  43 us
    all_to_all x1, waiting for transfers between devices, local(): lax.all_to_all(sent, 'kv', split_axis=0, concat_axis=0, tiled=True)  41.2 us
    pallas_call x1, Pallas kernels, local(): pl.pallas_call(attention_kernel, out_shape=(jax.ShapeDtypeStruct((DEVS, G...  13.7 us
    all_to_all x1, starting transfers between devices, local(): lax.all_to_all(outgoing, 'kv', split_axis=0, concat_axis=0, tiled=True)  13.5 us
    all_to_all x1, waiting for transfers between devices, local(): lax.all_to_all(terms, 'kv', 0, 0, tiled=True, axis_index_groups=same_core)  13.1 us
    all_to_all x1, starting transfers between devices, local(): lax.all_to_all(sent, 'kv', split_axis=0, concat_axis=0, tiled=True)  6.95 us
    ppermute x3, starting transfers between devices, local(): pieces.append(lax.ppermute(features, 'tp', ring))  4.9 us
    all_to_all x1, starting transfers between devices, local(): lax.all_to_all(terms, 'kv', 0, 0, tiled=True, axis_index_groups=same_core)  4.77 us
  transfers between devices with their start and end apart: 8, of which 5 were waited for; matrix products, arithmetic and copies ran while one was open for 7% of the time, Pallas kernels for 1%

profile of v3, /device:TPU:1, one launch (start us, length us, event | category | flops | bytes accessed | tf_op | source)
XLA Modules:
  0.0 170.4 jit_solution(4889781922723428421)
XLA Ops:
  0.6 0.8 select_reduce_fusion
  1.6 0.7 reduce_max.18.sel_ref
  2.3 3.0 %pack.1 = (bf16[64,2,64,128]{3,2,1,0:T(8,128)(2,1)}, bf16[2,6,64,128]{3,2,1,0:T(8,128)(2,1)}) custom-call(s32[2,64]{1,0:T(2,128)} %reduce_max.18.sel_ref, bf16[384,128]{1,0:T(8,128)(2,1)} %keys_ref.1, bf16[384,128]{1,0:T(8,128)(2,1)} %values_ref.1), custom_call_target="tpu_custom_call" | custom-call | flops 1000 | bytes 4194304 | tf_op jit(solution)/shard_map/pack/pallas_call | solution.py:214
  5.3 13.5 %all-to-all-start = ((bf16[64,2,64,128]{3,2,1,0:T(8,128)(2,1)}), bf16[64,2,64,128]{3,2,1,0:T(8,128)(2,1)}, u32[]{:S(2)}, u32[]{:S(2)}) async-start(bf16[64,2,64,128]{3,2,1,0:T(8,128)(2,1)} %get-tuple-element.12), calls=%async_computation | async-start | bytes 4194304 | tf_op jit(solution)/shard_map/all_to_all | solution.py:233
  18.8 0.9 select_select_fusion
  19.8 0.6 reshape.71.slot_ref
  20.5 0.6 reshape.72.near_ref
  21.1 0.4 reshape.73
  21.7 0.4 reshape.75
  22.3 1.1 pad.8.query_ref
  23.3 1.2 pad.9.grad_ref
  24.7 0.7 mul.20.sums_ref
  25.4 43.0 %all-to-all-done.remote_ref = bf16[64,2,64,128]{3,2,1,0:T(8,128)(2,1)} async-done(((bf16[64,2,64,128]{3,2,1,0:T(8,128)(2,1)}), bf16[64,2,64,128]{3,2,1,0:T(8,128)(2,1)}, u32[]{:S(2)}, u32[]{:S(2)}) %all-to-all-start) | async-done | bytes 2097184 | tf_op jit(solution)/shard_map/all_to_all | solution.py:233
  68.4 13.7 %attention.1 = (bf16[64,2,64,128]{3,2,1,0:T(8,128)(2,1)}, f32[2,6,64,128]{3,2,1,0:T(8,128)}, f32[12,64,256]{2,1,0:T(8,128)}) custom-call(s32[12,16]{1,0:T(8,128)} %reshape.71.slot_ref, s32[12,16]{1,0:T(8,128)} %reshape.72.near_ref, bf16[64,2,64,128]{3,2,1,0:T(8,128)(2,1)} %all-to-all-done.remote_ref, bf16[2,6,64,128]{3,2,1,0:T(8,128)(2,1)} %get-tuple-element.13.own_ref, ...), custom_call_target="tpu_custom_call" | custom-call | flops 4294967296 | bytes 8388608 | tf_op jit(solution)/shard_map/attention/pallas_call | solution.py:263
  82.0 6.9 %all-to-all-start.1 = ((bf16[64,2,64,128]{3,2,1,0:T(8,128)(2,1)}), bf16[64,2,64,128]{3,2,1,0:T(8,128)(2,1)S(1)}, u32[]{:S(2)}, u32[]{:S(2)}) async-start(bf16[64,2,64,128]{3,2,1,0:T(8,128)(2,1)} %get-tuple-element.15), calls=%async_computation.1 | async-start | bytes 4194304 | tf_op jit(solution)/shard_map/all_to_all | solution.py:282
  89.0 1.5 copy.25
  90.6 0.5 collective-permute-start.1
  91.2 1.3 collective-permute-done.1
  92.6 1.3 collective-permute-start.2
  93.9 2.5 %collective-permute-start.3 = (bf16[512,768]{1,0:T(8,128)(2,1)S(1)}, bf16[512,768]{1,0:T(8,128)(2,1)}, u32[]{:S(2)}, u32[]{:S(2)}) collective-permute-start(bf16[512,768]{1,0:T(8,128)(2,1)S(1)} %maximum_bitcast_fusion.refs_0_), channel_id=1, source_target_pairs={{0,2},{1,3},{2,0},{3,1},{4,6},{5,7},{6,4},{7,5},{8,10},{9,11},{10,... | collective-permute-start | bytes 2359304 | tf_op jit(solution)/shard_map/ppermute | solution.py:245
  96.3 1.2 collective-permute-start.4
  97.5 41.2 %all-to-all-done.1.returned_any = bf16[64,2,64,128]{3,2,1,0:T(8,128)(2,1)S(1)} async-done(((bf16[64,2,64,128]{3,2,1,0:T(8,128)(2,1)}), bf16[64,2,64,128]{3,2,1,0:T(8,128)(2,1)S(1)}, u32[]{:S(2)}, u32[]{:S(2)}) %all-to-all-start.1) | async-done | bytes 2097184 | tf_op jit(solution)/shard_map/all_to_all | solution.py:282
  138.7 2.2 %collect.1 = (f32[384,128]{1,0:T(8,128)}, f32[384,128]{1,0:T(8,128)}, bf16[384,128]{1,0:T(8,128)(2,1)S(1)}) custom-call(s32[2,64]{1,0:T(2,128)S(1)} %copy-done.1, bf16[64,2,64,128]{3,2,1,0:T(8,128)(2,1)S(1)} %all-to-all-done.1.returned_any, f32[2,6,64,128]{3,2,1,0:T(8,128)S(1)} %copy-done), custom_call_target="tpu_custom_call" | custom-call | flops 2097152 | bytes 4194304 | tf_op jit(solution)/shard_map/collect/pallas_call | solution.py:286
  140.9 2.3 %collective-permute-start = (bf16[384,128]{1,0:T(8,128)(2,1)S(1)}, bf16[384,128]{1,0:T(8,128)(2,1)S(1)}, u32[]{:S(2)}, u32[]{:S(2)}) collective-permute-start(bf16[384,128]{1,0:T(8,128)(2,1)S(1)} %get-tuple-element.19.near_ref), channel_id=1, source_target_pairs={{0,4},{4,0},{8,12},{12,8},{16,20},{20,16},{24,28},{28,24},{32,36},... | collective-permute-start | bytes 294920 | tf_op jit(solution)/shard_map/ppermute | solution.py:304
  143.3 0.9 collective-permute-done.far_ref
  144.2 3.1 %weights.1 = bf16[4,512,128]{2,1,0:T(8,128)(2,1)} custom-call(s32[1]{0:T(128)} %bitcast.6.tp_ref, bf16[384,128]{1,0:T(8,128)(2,1)S(1)} %get-tuple-element.19.near_ref, bf16[384,128]{1,0:T(8,128)(2,1)S(1)} %collective-permute-done.far_ref, bf16[512,768]{1,0:T(8,128)(2,1)S(1)} %maximum_bitcast_fusion.refs_0_, bf16[512,768]{1,0:T(8,128)(2,1)} %collective-permute-done.2.refs_1_, ...), custom_call_target="tpu_custom_call" | custom-call | flops 536870912 | bytes 4194304 | tf_op jit(solution)/shard_map/weights/pallas_call | solution.py:305
  147.4 4.8 %all-to-all-start.2 = ((bf16[32,64,128]{2,1,0:T(8,128)(2,1)}), bf16[32,64,128]{2,1,0:T(8,128)(2,1)}, u32[]{:S(2)}, u32[]{:S(2)}) async-start(bf16[32,64,128]{2,1,0:T(8,128)(2,1)} %bitcast.11), calls=%async_computation.2 | async-start | bytes 1048576 | tf_op jit(solution)/shard_map/all_to_all | solution.py:320
  152.1 0.7 reshape.77
  152.8 0.9 copy.24
  153.7 1.8 %reshape.78 = f32[384,512]{1,0:T(8,128)} reshape(f32[6,64,2,4,64]{4,3,2,1,0:T(4,128)S(1)} %copy.24) | data formatting | bytes 1572864 | tf_op jit(solution)/shard_map/reshape | solution.py:284
  155.5 13.1 %all-to-all-done.2 = bf16[32,64,128]{2,1,0:T(8,128)(2,1)} async-done(((bf16[32,64,128]{2,1,0:T(8,128)(2,1)}), bf16[32,64,128]{2,1,0:T(8,128)(2,1)}, u32[]{:S(2)}, u32[]{:S(2)}) %all-to-all-start.2) | async-done | bytes 524320 | tf_op jit(solution)/shard_map/all_to_all | solution.py:320
  168.7 1.7 %convert_reduce_fusion = f32[64,128]{1,0:T(8,128)} fusion(bf16[32,64,128]{2,1,0:T(8,128)(2,1)} %all-to-all-done.2), kind=kLoop, calls=%fused_computation | loop fusion | flops 516096 | bytes 557056 | tf_op jit(solution)/shard_map/reduce_sum | solution.py:321
  (25 shorter events, 0.9 us)
Async XLA Ops:
  5.3 15.8 %copy-start.3 = (bf16[384,512]{1,0:T(8,128)(2,1)S(1)}, bf16[384,512]{1,0:T(8,128)(2,1)}, u32[]{:S(2)}) copy-start(bf16[384,512]{1,0:T(8,128)(2,1)} %param.7) | copy-start | bytes 1179652
  5.3 63.1 %all-to-all-start = ((bf16[64,2,64,128]{3,2,1,0:T(8,128)(2,1)}), bf16[64,2,64,128]{3,2,1,0:T(8,128)(2,1)}, u32[]{:S(2)}, u32[]{:S(2)}) async-start(bf16[64,2,64,128]{3,2,1,0:T(8,128)(2,1)} %get-tuple-element.12), calls=%async_computation | async-start | bytes 4194304 | tf_op jit(solution)/shard_map/all_to_all | solution.py:233
  18.8 2.9 %copy-start.4 = (bf16[384,512]{1,0:T(8,128)(2,1)S(1)}, bf16[384,512]{1,0:T(8,128)(2,1)}, u32[]{:S(2)}) copy-start(bf16[384,512]{1,0:T(8,128)(2,1)} %param.11) | copy-start | bytes 1179652
  22.3 2.3 %copy-start.5 = (f32[8,384]{1,0:T(8,128)S(1)}, f32[8,384]{1,0:T(8,128)}, u32[]{:S(2)}) copy-start(f32[8,384]{1,0:T(8,128)} %param.10) | copy-start | bytes 36868
  82.0 56.7 %all-to-all-start.1 = ((bf16[64,2,64,128]{3,2,1,0:T(8,128)(2,1)}), bf16[64,2,64,128]{3,2,1,0:T(8,128)(2,1)S(1)}, u32[]{:S(2)}, u32[]{:S(2)}) async-start(bf16[64,2,64,128]{3,2,1,0:T(8,128)(2,1)} %get-tuple-element.15), calls=%async_computation.1 | async-start | bytes 4194304 | tf_op jit(solution)/shard_map/all_to_all | solution.py:282
  90.5 48.2 %copy-start = (f32[2,6,64,128]{3,2,1,0:T(8,128)S(1)}, f32[2,6,64,128]{3,2,1,0:T(8,128)}, u32[]{:S(2)}) copy-start(f32[2,6,64,128]{3,2,1,0:T(8,128)} %get-tuple-element.16.kept_ref) | copy-start | bytes 1179652
  90.5 48.2 %copy-start.1 = (s32[2,64]{1,0:T(2,128)S(1)}, s32[2,64]{1,0:T(2,128)}, u32[]{:S(2)}) copy-start(s32[2,64]{1,0:T(2,128)} %reduce_max.18.sel_ref) | copy-start | bytes 1540
  90.6 1.9 %collective-permute-start.1 = (bf16[384,512]{0,1:T(8,128)(2,1)S(1)}, bf16[384,512]{0,1:T(8,128)(2,1)S(1)}, u32[]{:S(2)}, u32[]{:S(2)}) collective-permute-start(bf16[384,512]{0,1:T(8,128)(2,1)S(1)} %bitcast.20), channel_id=1, source_target_pairs={{0,4},{4,0},{8,12},{12,8},{16,20},{20,16},{24,28},{28,24},{32,36},... | collective-permute-start | bytes 1179656 | tf_op jit(solution)/shard_map/ppermute | solution.py:241
  92.6 50.7 %collective-permute-start.2 = (bf16[512,768]{1,0:T(8,128)(2,1)S(1)}, bf16[512,768]{1,0:T(8,128)(2,1)}, u32[]{:S(2)}, u32[]{:S(2)}) collective-permute-start(bf16[512,768]{1,0:T(8,128)(2,1)S(1)} %maximum_bitcast_fusion.refs_0_), channel_id=1, source_target_pairs={{0,1},{1,2},{2,3},{3,0},{4,5},{5,6},{6,7},{7,4},{8,9},{9,10},{10,1... | collective-permute-start | bytes 2359304 | tf_op jit(solution)/shard_map/ppermute | solution.py:245
  93.9 49.4 %collective-permute-start.3 = (bf16[512,768]{1,0:T(8,128)(2,1)S(1)}, bf16[512,768]{1,0:T(8,128)(2,1)}, u32[]{:S(2)}, u32[]{:S(2)}) collective-permute-start(bf16[512,768]{1,0:T(8,128)(2,1)S(1)} %maximum_bitcast_fusion.refs_0_), channel_id=1, source_target_pairs={{0,2},{1,3},{2,0},{3,1},{4,6},{5,7},{6,4},{7,5},{8,10},{9,11},{10,... | collective-permute-start | bytes 2359304 | tf_op jit(solution)/shard_map/ppermute | solution.py:245
  96.3 47.0 %collective-permute-start.4 = (bf16[512,768]{1,0:T(8,128)(2,1)S(1)}, bf16[512,768]{1,0:T(8,128)(2,1)}, u32[]{:S(2)}, u32[]{:S(2)}) collective-permute-start(bf16[512,768]{1,0:T(8,128)(2,1)S(1)} %maximum_bitcast_fusion.refs_0_), channel_id=1, source_target_pairs={{0,3},{1,0},{2,1},{3,2},{4,7},{5,4},{6,5},{7,6},{8,11},{9,8},{10,9... | collective-permute-start | bytes 2359304 | tf_op jit(solution)/shard_map/ppermute | solution.py:245
  140.9 3.3 %collective-permute-start = (bf16[384,128]{1,0:T(8,128)(2,1)S(1)}, bf16[384,128]{1,0:T(8,128)(2,1)S(1)}, u32[]{:S(2)}, u32[]{:S(2)}) collective-permute-start(bf16[384,128]{1,0:T(8,128)(2,1)S(1)} %get-tuple-element.19.near_ref), channel_id=1, source_target_pairs={{0,4},{4,0},{8,12},{12,8},{16,20},{20,16},{24,28},{28,24},{32,36},... | collective-permute-start | bytes 294920 | tf_op jit(solution)/shard_map/ppermute | solution.py:304
  147.3 4.8 %copy-start.2 = (f32[12,64,256]{2,1,0:T(8,128)S(1)}, f32[12,64,256]{2,1,0:T(8,128)}, u32[]{:S(2)}) copy-start(f32[12,64,256]{2,1,0:T(8,128)} %get-tuple-element.14) | copy-start | bytes 2359300
  147.4 21.3 %all-to-all-start.2 = ((bf16[32,64,128]{2,1,0:T(8,128)(2,1)}), bf16[32,64,128]{2,1,0:T(8,128)(2,1)}, u32[]{:S(2)}, u32[]{:S(2)}) async-start(bf16[32,64,128]{2,1,0:T(8,128)(2,1)} %bitcast.11), calls=%async_computation.2 | async-start | bytes 1048576 | tf_op jit(solution)/shard_map/all_to_all | solution.py:320
